TPU v7x, 512 devices: a whole 4x4x16 slice. The times are simulated.
512 devices in a mesh: sp: 32 (over z, core), tp: 16 (over y, x).
Axes of the slice: x: 4, y: 4, z: 16, core: 2. Of those that a mesh axis runs over, the one named last changes fastest.
Arguments:
- tokens: bfloat16 [6144, 4096], P('sp', 'tp'), may hold values from -60 to 60
- lean_query: bfloat16 [6144, 16, 64], P('sp', 'tp'), may hold values from -6 to 6
- lean_key: bfloat16 [6144, 2, 64], P('sp'), may hold values from -6 to 6
- lean_value: bfloat16 [6144, 2, 64], P('sp'), may hold values from -6 to 6
- lean_gains: float32 [2, 64], replicated, may hold values from 0.25 to 7.5
- broad_query: bfloat16 [6144, 16, 128], P('sp', 'tp'), may hold values from -6 to 6
- broad_key: bfloat16 [6144, 2, 128], P('sp'), may hold values from -6 to 6
- broad_value: bfloat16 [6144, 2, 128], P('sp'), may hold values from -6 to 6
- broad_gains: float32 [2, 128], replicated, may hold values from 0.25 to 7.5
- mixer_gain: float32 [3072], replicated, may hold values from 0.1 to 1.9
- output_weight: bfloat16 [3072, 4096], P(None, 'tp'), may hold values from -0.109375 to 0.109375
- channel_gain: float32 [4096], P('tp'), may hold values from 0.1 to 1.9
- gate_weight: bfloat16 [32, 4096, 2048], P('sp', None, 'tp'), may hold values from -0.09375 to 0.09375
- up_weight: bfloat16 [32, 4096, 2048], P('sp', None, 'tp'), may hold values from -0.09375 to 0.09375
- down_weight: bfloat16 [32, 2048, 4096], P('sp', None, 'tp'), may hold values from -0.125 to 0.125
- route_experts: int32 [6144, 2], P('sp'), may hold values from 0 to 31, as said below
- route_logits: float32 [6144, 2], P('sp'), may hold values from -6 to 6
- group_weight: float32 [6144], P('sp'), may hold values from 0.3 to 1
Outputs:
- encoded: bfloat16 [6144, 4096], P('sp', 'tp')
Inputs may be any that keep to these rules, and one draw needn't show every extreme that they name: `route_experts`: each row names two different experts of one group, expert e lying in group e // 8. In every aligned block of 192 rows no expert is named by more than 24 rows; one group, the same for all blocks, is named by exactly half of each block's rows, and each of its experts by exactly 24 of them.
All inputs are finite; a program needn't handle non-finite values.
Results may differ from a plain program's by a relative error of at most 0.0083.
Values may be sent and summed in bfloat16 or wider, within the bound.
A program may use at most 64 MiB of HBM per device.

v0:
```python
import jax
import jax.numpy as jnp
from jax import lax
from jax.sharding import Mesh
from jax.sharding import PartitionSpec as P

D = 4096
HQ_A = 16
KV_A = 2
HQ_B = 16
KV_B = 2
GRID_W = 64
GROUPS = 4
TP = ("tp_0", "tp_1")


epsilon = 1e-06
theta_base = 10000.0
floor_score = -1e30


def sent_together(arrays, axis, dim, along):
    ends, at = ([], 0)
    for a in arrays[:-1]:
        at += a.shape[along]
        ends.append(at)
    both = jnp.concatenate(arrays, axis=along)
    return tuple(jnp.split(lax.all_gather(both, axis, axis=dim, tiled=True), ends, axis=along))


def sent_to_all(shard, axis):
    copies = jnp.broadcast_to(shard, (lax.axis_size(axis), *shard.shape))
    return lax.all_to_all(copies, axis, split_axis=0, concat_axis=0, tiled=True)


def over_copies(shard, axis):
    return sent_to_all(shard, axis).sum(axis=0)


def gather_axes(shard, axes, dim):
    for axis in reversed(axes):
        shard = lax.all_gather(shard, axis, axis=dim, tiled=True)
    return shard


def axial_angles(positions, head_size):
    quarter = head_size // 4
    frequency = theta_base ** (-jnp.arange(quarter, dtype=jnp.float32) / quarter)
    grid_rows = (positions // GRID_W).astype(jnp.float32)
    grid_columns = (positions % GRID_W).astype(jnp.float32)
    return (grid_rows[:, None] * frequency[None, :], grid_columns[:, None] * frequency[None, :])


def turn_half(values, angles):
    half_width = values.shape[-1] // 2
    first_half = values[..., :half_width]
    second = values[..., half_width:]
    cosine = jnp.cos(angles)[:, None, :]
    sine_part = jnp.sin(angles)[:, None, :]
    return jnp.concatenate(
        [first_half * cosine - second * sine_part, second * cosine + first_half * sine_part],
        axis=-1,
    )


def prepare(raw_values, gain_row, positions):
    values = raw_values.astype(jnp.float32)
    values = (
        values * lax.rsqrt(jnp.mean(values * values, axis=-1, keepdims=True) + epsilon) * gain_row
    )
    row_angles, column_angles = axial_angles(positions, raw_values.shape[-1])
    half_width = raw_values.shape[-1] // 2
    turned = jnp.concatenate(
        [
            turn_half(values[..., :half_width], row_angles),
            turn_half(values[..., half_width:], column_angles),
        ],
        axis=-1,
    )
    return turned.astype(jnp.bfloat16)


def group_norm(head_rows, gain_row):
    values = head_rows.astype(jnp.float32)
    return (
        values * lax.rsqrt(jnp.mean(values * values, axis=-1, keepdims=True) + epsilon) * gain_row
    ).astype(jnp.bfloat16)


def own_heads(query_raw, key_raw, value_raw, gain_pair, positions, lane_index, group_ratio):
    head_count, head_size = (query_raw.shape[1], query_raw.shape[2])
    key_heads = max(1, head_count // group_ratio)
    kv_start = lane_index * head_count // group_ratio
    key_part = lax.dynamic_slice_in_dim(key_raw, kv_start, key_heads, 1)
    value_part = lax.dynamic_slice_in_dim(value_raw, kv_start, key_heads, 1)
    queries = prepare(query_raw, gain_pair[0], positions).reshape(
        query_raw.shape[0], key_heads, head_count // key_heads, head_size
    )
    return (queries, prepare(key_part, gain_pair[1], positions), value_part)


def start_state(queries):
    row_count = queries.shape[0]
    head_count = queries.shape[1] * queries.shape[2]
    return (
        jnp.full((head_count, row_count), floor_score, jnp.float32),
        jnp.zeros((head_count, row_count), jnp.float32),
        jnp.zeros((row_count, head_count, queries.shape[3]), jnp.float32),
    )


def attend_piece(fold_state, queries, keys, values):
    peak_score, weight_sum, accumulated = fold_state
    row_count, key_heads, grouped, head_size = queries.shape
    key_count = keys.shape[0]
    scores = jnp.einsum(
        "qkgd,skd->kgqs", queries, keys, preferred_element_type=jnp.float32
    ) * head_size ** (-0.5)
    scores = scores.reshape(key_heads * grouped, row_count, key_count)
    new_peak = jnp.maximum(peak_score, jnp.max(scores, axis=-1))
    weights = jnp.exp(scores - new_peak[..., None])
    new_sum = jnp.sum(weights, axis=-1)
    rounded = weights.astype(jnp.bfloat16).reshape(key_heads, grouped, row_count, key_count)
    partial_value = jnp.einsum(
        "kgqs,skd->qkgd", rounded, values, preferred_element_type=jnp.float32
    )
    partial_value = partial_value.reshape(row_count, key_heads * grouped, head_size)
    return (new_peak, new_sum, partial_value)


def finish_heads(fold_state):
    accumulated = fold_state[2]
    return (
        (accumulated / jnp.transpose(fold_state[1])[:, :, None])
        .astype(jnp.bfloat16)
        .reshape(accumulated.shape[0], -1)
    )


def on_device(
    tokens,
    lean_query,
    lean_key,
    lean_value,
    lean_gains,
    broad_query,
    broad_key,
    broad_value,
    broad_gains,
    mixer_gain,
    output_weight,
    channel_gain,
    gate_weight,
    up_weight,
    down_weight,
    route_experts,
    route_logits,
    group_weight,
):
    row_count = tokens.shape[0]
    positions = lax.axis_index("sp") * row_count + jnp.arange(row_count, dtype=jnp.int32)
    lane_index = lax.axis_index(TP)
    lean_queries, lean_keys, lean_values = own_heads(
        lean_query, lean_key, lean_value, lean_gains, positions, lane_index, HQ_A // KV_A
    )
    broad_queries, broad_keys, broad_values = own_heads(
        broad_query, broad_key, broad_value, broad_gains, positions, lane_index, HQ_B // KV_B
    )
    shard_rows = sent_together((lean_keys, lean_values, broad_keys, broad_values), "sp", 0, 2)
    lean_state = attend_piece(start_state(lean_queries), lean_queries, shard_rows[0], shard_rows[1])
    broad_state = attend_piece(
        start_state(broad_queries), broad_queries, shard_rows[2], shard_rows[3]
    )
    lean_all, broad_all = (
        lax.all_gather(finish_heads(lean_state), TP, axis=1, tiled=True),
        lax.all_gather(finish_heads(broad_state), TP, axis=1, tiled=True),
    )
    lean_width = lean_all.shape[1]
    stream = tokens.astype(jnp.float32) + jnp.dot(
        group_norm(lean_all, mixer_gain[:lean_width]),
        output_weight[:lean_width],
        preferred_element_type=jnp.float32,
    )
    stream = stream + jnp.dot(
        group_norm(broad_all, mixer_gain[lean_width:]),
        output_weight[lean_width:],
        preferred_element_type=jnp.float32,
    )
    squares = over_copies(jnp.sum(stream * stream, axis=1), TP)
    normed = (stream * lax.rsqrt(squares / D + epsilon)[:, None] * channel_gain).astype(
        jnp.bfloat16
    )
    experts = lax.axis_size("sp")
    capacity = row_count // (experts // GROUPS)
    flat_experts = route_experts.reshape(-1)
    onehot = (flat_experts[:, None] == jnp.arange(experts, dtype=jnp.int32)[None, :]).astype(
        jnp.int32
    )
    slot_rank = jnp.sum((jnp.cumsum(onehot, axis=0) - 1) * onehot, axis=1)
    slot_index = flat_experts * capacity + slot_rank
    token_owner = jnp.repeat(jnp.arange(row_count, dtype=jnp.int32), route_experts.shape[1])
    filled = jnp.zeros((experts * capacity,), jnp.int32).at[slot_index].set(token_owner + 1)
    slot_live = (filled > 0)[:, None]
    source = jnp.maximum(filled - 1, 0)
    outgoing = jnp.where(slot_live, normed[source], jnp.zeros((), jnp.bfloat16)).reshape(
        experts, capacity, -1
    )
    arrived = lax.all_to_all(outgoing, "sp", split_axis=0, concat_axis=0, tiled=True)
    sources = arrived.shape[0]
    item_count = arrived.shape[1]
    shard_rows = lax.all_gather(arrived, TP, axis=2, tiled=True)
    flat_rows = shard_rows.reshape(sources * item_count, shard_rows.shape[2])
    gate_part = gate_weight[0]
    up_part = up_weight[0]
    gate_value = jnp.dot(flat_rows, gate_part, preferred_element_type=jnp.float32)
    up_value = jnp.dot(flat_rows, up_part, preferred_element_type=jnp.float32)
    hidden = (jax.nn.silu(gate_value) * up_value).astype(jnp.bfloat16)
    down_part = down_weight[0]
    result = jnp.dot(gather_axes(hidden, TP, 1), down_part, preferred_element_type=jnp.float32)
    result = result.astype(jnp.bfloat16).reshape(sources, item_count, -1)
    returned = lax.all_to_all(result, "sp", split_axis=0, concat_axis=0, tiled=True)
    picked = (
        returned.reshape(experts * capacity, -1)[slot_index]
        .reshape(row_count, route_experts.shape[1], -1)
        .astype(jnp.float32)
    )
    logit_gap = route_logits[:, 0] - route_logits[:, 1]
    weights = group_weight[:, None] * jax.nn.sigmoid(jnp.stack([logit_gap, -logit_gap], axis=1))
    return (stream + jnp.sum(picked * weights[:, :, None], axis=1)).astype(jnp.bfloat16)


def solution(mesh):
    finer = Mesh(mesh.devices.reshape(mesh.shape["sp"], 4, 4), ("sp", "tp_0", "tp_1"))
    return jax.shard_map(
        on_device,
        mesh=finer,
        in_specs=(
            P("sp", TP),
            P("sp", TP, None),
            P("sp", None, None),
            P("sp", None, None),
            P(),
            P("sp", TP, None),
            P("sp", None, None),
            P("sp", None, None),
            P(),
            P(),
            P(None, TP),
            P(TP),
            P("sp", None, TP),
            P("sp", None, TP),
            P("sp", None, TP),
            P("sp", None),
            P("sp", None),
            P("sp"),
        ),
        out_specs=P("sp", TP),
        check_vma=False,
    )
```

profile of v0, /device:TPU:1, one launch (start us, length us, event | category | flops | bytes accessed | tf_op | source)
XLA Modules:
  0.0 401.3 jit_solution(2355474312240719363)
XLA Ops:
  6.6 0.8 slice_bitcast_fusion.21
  7.4 0.8 fusion.57
  8.1 0.8 fusion.59
  9.0 0.9 fusion.58
  9.8 0.2 fusion.137
  10.1 0.1 copy.95
  10.2 0.1 copy.96
  10.3 0.1 copy.97
  10.4 0.1 copy.98
  10.5 0.8 constant_dynamic-slice_fusion.2
  11.3 0.1 copy.113
  11.4 1.2 constant_dynamic-slice_fusion
  12.6 0.1 copy.114
  12.7 0.8 slice_bitcast_fusion.20
  13.5 0.9 copy.105
  14.6 0.3 fusion.98
  15.0 0.1 copy.99
  15.1 0.1 copy.100
  15.2 0.1 copy.101
  15.3 0.1 copy.102
  15.5 0.9 concatenate.60
  16.4 0.8 copy.107
  17.2 0.1 eq.30
  17.3 0.1 eq.34
  17.4 0.7 broadcast_multiply_fusion
  18.1 0.1 copy.106
  18.3 0.1 mul.525
  18.4 0.9 reduce-window.6
  19.3 0.2 slice_reduce_fusion
  19.6 0.1 reshape.958
  19.8 2.9 scatter_custom_fusion
  22.8 73.3 %all-gather.4.cloned.1.call-done = bf16[6144,1,384]{2,0,1:T(8,128)(2,1)} async-done(((bf16[192,1,384]{2,0,1:T(8,128)(2,1)}), bf16[6144,1,384]{2,0,1:T(8,128)(2,1)}) %all-gather.4.cloned.1.call-update) | async-done | bytes 4718608 | tf_op jit(solution)/shard_map/all_gather | solution.py:28
  96.1 2.5 fusion.163
  98.6 0.8 fusion.3
  99.4 1.6 fusion.29
  101.0 18.8 %all_gather.19 = bf16[192,1024]{0,1:T(8,128)(2,1)S(1)} all-gather(bf16[192,64]{0,1:T(8,128)(2,1)S(1)} %fusion.29), channel_id=1, replica_groups=mesh['sp'=32,'tp_0'=4,'tp_1'=4] {'tp_0','tp_1'}, dimensions={1}, use_global_device_ids=true | all-gather | bytes 417792 | tf_op jit(solution)/shard_map/all_gather | solution.py:175
  119.8 0.2 fusion.38
  120.0 0.9 fusion.164
  121.0 0.8 fusion.1
  121.8 0.9 fusion.35
  122.8 19.2 %all_gather.20 = bf16[192,2048]{1,0:T(8,128)(2,1)S(1)} all-gather(bf16[192,128]{1,0:T(8,128)(2,1)S(1)} %fusion.35), channel_id=1, replica_groups=mesh['sp'=32,'tp_0'=4,'tp_1'=4] {'tp_0','tp_1'}, dimensions={1}, use_global_device_ids=true | all-gather | bytes 835584 | tf_op jit(solution)/shard_map/all_gather | solution.py:176
  141.9 0.2 fusion.16
  142.2 0.5 convolution_add_fusion.1
  142.7 0.5 multiply_reduce_fusion.1
  143.3 0.6 broadcast_in_dim.19
  143.9 3.8 all-to-all-start
  147.7 0.2 all-gather.6.cloned.1.call-start
  148.0 6.1 %all-to-all-done = f32[16,1,192]{2,1,0:T(1,128)S(1)} async-done(((f32[16,1,192]{2,1,0:T(1,128)}), f32[16,1,192]{2,1,0:T(1,128)S(1)}, u32[]{:S(2)}, u32[]{:S(2)}) %all-to-all-start) | async-done | bytes 12320 | tf_op jit(solution)/shard_map/all_to_all | solution.py:33
  154.3 2.7 gather_fusion
  156.9 0.2 broadcast_select_fusion
  157.1 48.3 %all_to_all.16 = bf16[32,24,256]{2,1,0:T(8,128)(2,1)} all-to-all(bf16[32,24,256]{2,1,0:T(8,128)(2,1)S(1)} %broadcast_select_fusion), channel_id=1, replica_groups=mesh['sp'=32,'tp_0'=4,'tp_1'=4] {'sp'}, dimensions={0} | all-to-all | bytes 786432 | tf_op jit(solution)/shard_map/all_to_all | solution.py:208
  205.5 68.6 %all-gather.6.cloned.1.call-done = bf16[32,24,4096]{2,1,0:T(8,128)(2,1)} async-done(((bf16[32,24,256]{2,1,0:T(8,128)(2,1)}), bf16[32,24,4096]{2,1,0:T(8,128)(2,1)}) %all-gather.6.cloned.1.call-update) | async-done | bytes 6291472 | tf_op jit(solution)/shard_map/all_gather | solution.py:211
  274.1 4.7 %fusion.43 = f32[768,128]{1,0:T(8,128)S(1)} fusion(bf16[768,4096]{1,0:T(8,128)(2,1)} %bitcast.177, bf16[1,4096,128]{2,1,0:T(8,128)(2,1)S(1)} %copy-done.6), kind=kOutput, calls=%fused_computation.50 | convolution fusion | flops 805306368 | bytes 7733248 | tf_op jit(solution)/shard_map/dot_general | solution.py:215
  278.8 3.0 fusion.19
  281.8 15.7 %all_gather.22 = bf16[768,512]{1,0:T(8,128)(2,1)} all-gather(bf16[768,128]{1,0:T(8,128)(2,1)S(1)} %fusion.19), channel_id=1, replica_groups=mesh['sp'=32,'tp_0'=4,'tp_1'=4] {'tp_1'}, dimensions={1}, use_global_device_ids=true | all-gather | bytes 983040 | tf_op jit(solution)/shard_map/all_gather | solution.py:42
  297.6 49.1 %all-gather.8.cloned.1.call-done = bf16[768,2048]{1,0:T(8,128)(2,1)} async-done(((bf16[768,512]{1,0:T(8,128)(2,1)}), bf16[768,2048]{1,0:T(8,128)(2,1)}) %all-gather.8.cloned.1.call-update) | async-done | bytes 3145744 | tf_op jit(solution)/shard_map/all_gather | solution.py:42
  346.7 3.6 convolution_convert_fusion
  350.4 13.2 %all-to-all-start.2 = ((bf16[32,24,256]{2,1,0:T(8,128)(2,1)}), bf16[32,24,256]{2,1,0:T(8,128)(2,1)S(1)}, u32[]{:S(2)}, u32[]{:S(2)}) async-start(bf16[32,24,256]{2,1,0:T(8,128)(2,1)} %bitcast.38), calls=%async_computation.2 | async-start | bytes 786432 | tf_op jit(solution)/shard_map/all_to_all | solution.py:221
  363.6 0.1 copy.111
  363.7 27.6 %all-to-all-done.2 = bf16[32,24,256]{2,1,0:T(8,128)(2,1)S(1)} async-done(((bf16[32,24,256]{2,1,0:T(8,128)(2,1)}), bf16[32,24,256]{2,1,0:T(8,128)(2,1)S(1)}, u32[]{:S(2)}, u32[]{:S(2)}) %all-to-all-start.2) | async-done | bytes 393248 | tf_op jit(solution)/shard_map/all_to_all | solution.py:221
  391.3 2.0 gather_fusion.1
  393.4 0.2 reshape.937
  393.6 0.5 multiply_reduce_fusion
  394.1 0.7 add_convert_fusion
  (61 shorter events, 1.0 us)
Async XLA Ops:
  6.5 340.2 %copy-start = (bf16[1,2048,256]{2,1,0:T(8,128)(2,1)S(1)}, bf16[1,2048,256]{2,1,0:T(8,128)(2,1)}, u32[]{:S(2)}) copy-start(bf16[1,2048,256]{2,1,0:T(8,128)(2,1)} %param.32) | copy-start | bytes 3145732
  6.5 89.6 %all-gather.4.cloned.1.call-start = ((), (), s32[]{:S(2)}) async-start(), calls=%async_computation.3 | async-start | bytes 4866048 | tf_op jit(solution)/shard_map/all_gather | solution.py:28
  96.1 3.3 slice-start
  96.1 3.3 slice-start.1
  121.8 20.4 %slice-start.2 = ((f32[3072]{0:T(1024)}), f32[1024]{0:T(1024)S(1)}, s32[]{:S(2)}) async-start(f32[3072]{0:T(1024)} %param.27), calls=%async_computation.8 | async-start | bytes 8192 | tf_op jit(solution)/shard_map/slice | solution.py:180
  121.8 20.4 %copy-start.5 = (bf16[3072,256]{1,0:T(8,128)(2,1)S(1)}, bf16[3072,256]{1,0:T(8,128)(2,1)}, u32[]{:S(2)}) copy-start(bf16[3072,256]{1,0:T(8,128)(2,1)} %param.28) | copy-start | bytes 4718596
  121.8 20.4 %copy-start.7 = (bf16[192,256]{1,0:T(8,128)(2,1)S(1)}, bf16[192,256]{1,0:T(8,128)(2,1)}, u32[]{:S(2)}) copy-start(bf16[192,256]{1,0:T(8,128)(2,1)} %param.18) | copy-start | bytes 294916
  121.8 20.9 %slice-start.3 = ((f32[3072]{0:T(1024)}), f32[2048]{0:T(1024)S(1)}, s32[]{:S(2)}) async-start(f32[3072]{0:T(1024)} %param.27), calls=%async_computation.9 | async-start | bytes 16384 | tf_op jit(solution)/shard_map/slice | solution.py:185
  122.8 31.4 %copy-start.2 = (f32[256]{0:T(256)S(1)}, f32[256]{0:T(256)}, u32[]{:S(2)}) copy-start(f32[256]{0:T(256)} %param.29) | copy-start | bytes 3076
  142.7 131.3 %copy-start.6 = (bf16[1,4096,128]{2,1,0:T(8,128)(2,1)S(1)}, bf16[1,4096,128]{2,1,0:T(8,128)(2,1)}, u32[]{:S(2)}) copy-start(bf16[1,4096,128]{2,1,0:T(8,128)(2,1)} %param.30) | copy-start | bytes 3145732
  143.9 10.2 %all-to-all-start = ((f32[16,1,192]{2,1,0:T(1,128)}), f32[16,1,192]{2,1,0:T(1,128)S(1)}, u32[]{:S(2)}, u32[]{:S(2)}) async-start(f32[16,1,192]{2,1,0:T(1,128)} %broadcast_in_dim.19), calls=%async_computation | async-start | bytes 32768 | tf_op jit(solution)/shard_map/all_to_all | solution.py:33
  147.7 126.4 %all-gather.6.cloned.1.call-start = ((), (), s32[]{:S(2)}) async-start(), calls=%async_computation.4 | async-start | bytes 6684672 | tf_op jit(solution)/shard_map/all_gather | solution.py:211
  205.5 141.3 %all-gather.8.cloned.1.call-start = ((), (), s32[]{:S(2)}) async-start(), calls=%async_computation.5 | async-start | bytes 3932160 | tf_op jit(solution)/shard_map/all_gather | solution.py:42
  274.1 4.7 %copy-start.4 = (bf16[32,24,4096]{2,1,0:T(8,128)(2,1)S(1)}, bf16[32,24,4096]{2,1,0:T(8,128)(2,1)}, u32[]{:S(2)}) copy-start(bf16[32,24,4096]{2,1,0:T(8,128)(2,1)} %all-gather.6.cloned.1.call-done) | copy-start | bytes 18874372
  297.6 66.0 %copy-start.1 = (f32[192,2]{0,1:T(2,128)S(1)}, f32[192,2]{0,1:T(2,128)}, u32[]{:S(2)}) copy-start(f32[192,2]{0,1:T(2,128)} %param.34) | copy-start | bytes 4612
  297.6 66.0 %copy-start.3 = (f32[192]{0:T(256)S(1)}, f32[192]{0:T(256)}, u32[]{:S(2)}) copy-start(f32[192]{0:T(256)} %param.35) | copy-start | bytes 2308
  350.4 40.9 %all-to-all-start.2 = ((bf16[32,24,256]{2,1,0:T(8,128)(2,1)}), bf16[32,24,256]{2,1,0:T(8,128)(2,1)S(1)}, u32[]{:S(2)}, u32[]{:S(2)}) async-start(bf16[32,24,256]{2,1,0:T(8,128)(2,1)} %bitcast.38), calls=%async_computation.2 | async-start | bytes 786432 | tf_op jit(solution)/shard_map/all_to_all | solution.py:221
Sparse Core Ops, SparseCore 0:
  16.5 79.6 all-gather.3
  205.6 68.4 all-gather.5
  297.7 48.9 all-gather.7
where the time goes:
time: 402 us; the launch traced here: 401 us
  waiting for transfers between devices  225 us (56%)
  blocking collectives  102 us (25%)
  matrix products  18.3 us (5%)
  starting transfers between devices  17.2 us (4%)
  local copies, waits for them, and re-layouts  16.8 us (4%)
  between operations  13.6 us (3%)
  other arithmetic  8.63 us (2%)
    all_gather x1, waiting for transfers between devices, sent_together(): lax.all_gather(both, axis, axis=dim, tiled=True)  73.3 us
    all_gather x1, waiting for transfers between devices, on_device(): shard_rows = lax.all_gather(arrived, TP, axis=2, tiled=True)  68.6 us
    all_gather x1, waiting for transfers between devices, gather_axes(): shard = lax.all_gather(shard, axis, axis=dim, tiled=True)  49.1 us
    all_to_all x1, blocking collectives, on_device(): lax.all_to_all(outgoing, 'sp', split_axis=0, concat_axis=0, tiled=True)  48.3 us
    all_to_all x1, waiting for transfers between devices, on_device(): lax.all_to_all(result, 'sp', split_axis=0, concat_axis=0, tiled=True)  27.6 us
    all_gather x1, blocking collectives, on_device(): lax.all_gather(finish_heads(broad_state), TP, axis=1, tiled=True)  19.2 us
    all_gather x1, blocking collectives, on_device(): lax.all_gather(finish_heads(lean_state), TP, axis=1, tiled=True)  18.8 us
    all_gather x1, blocking collectives, gather_axes(): shard = lax.all_gather(shard, axis, axis=dim, tiled=True)  15.7 us
  transfers between devices with their start and end apart: 5, of which 5 were waited for; matrix products, arithmetic and copies ran while one was open for 2% of the time, Pallas kernels for 0%

commit v1 on v0

v1 whole, which is shorter than its diff:
```python
import functools
import math

import jax
import jax.numpy as jnp
from jax import lax
from jax.experimental import pallas as pl
from jax.experimental.pallas import tpu as pltpu
from jax.sharding import Mesh
from jax.sharding import PartitionSpec as P

D = 4096
GRID_W = 64
KV = 2
GROUPS = 4
NY, NX = 4, 4
NCH = 4
HA, HB = 64, 128
FW = 256
FE = 128
MESH = pl.DeviceIdType.MESH
epsilon = 1e-06
theta_base = 10000.0
LOG2E = 1.4426950408889634


def axial_angles(positions, head_size):
    quarter = head_size // 4
    frequency = theta_base ** (-jnp.arange(quarter, dtype=jnp.float32) / quarter)
    grid_rows = (positions // GRID_W).astype(jnp.float32)
    grid_columns = (positions % GRID_W).astype(jnp.float32)
    return (grid_rows[:, None] * frequency[None, :], grid_columns[:, None] * frequency[None, :])


def turn_half(values, angles):
    half_width = values.shape[-1] // 2
    first_half = values[..., :half_width]
    second = values[..., half_width:]
    cosine = jnp.cos(angles)
    sine_part = jnp.sin(angles)
    return jnp.concatenate(
        [first_half * cosine - second * sine_part, second * cosine + first_half * sine_part],
        axis=-1,
    )


def prepare(raw_values, gain_row, positions):
    values = raw_values.astype(jnp.float32)
    values = (
        values * lax.rsqrt(jnp.mean(values * values, axis=-1, keepdims=True) + epsilon) * gain_row
    )
    row_angles, column_angles = axial_angles(positions, raw_values.shape[-1])
    half_width = raw_values.shape[-1] // 2
    turned = jnp.concatenate(
        [
            turn_half(values[..., :half_width], row_angles),
            turn_half(values[..., half_width:], column_angles),
        ],
        axis=-1,
    )
    return turned.astype(jnp.bfloat16)


def rcopy(src, dst, send_sem, recv_sem, device):
    return pltpu.make_async_remote_copy(
        src_ref=src,
        dst_ref=dst,
        send_sem=send_sem,
        recv_sem=recv_sem,
        device_id=device,
        device_id_type=MESH,
    )


def landed(ref, sem):
    pltpu.make_async_copy(ref, ref, sem).wait()


def dot_t(a, b):
    return lax.dot_general(a, b, (((1,), (1,)), ((), ())), preferred_element_type=jnp.float32)


def dot_n(a, b):
    return jnp.dot(a, b, preferred_element_type=jnp.float32)


def dot_exact(a, b, dims):
    return lax.dot_general(
        a,
        b,
        (dims, ((), ())),
        preferred_element_type=jnp.float32,
        precision=lax.Precision.HIGHEST,
    )


def layer_kernel(
    dims,
    q_ref,
    kv_ref,
    tok_ref,
    wl_ref,
    wb_ref,
    gate_ref,
    up_ref,
    down_ref,
    mg_ref,
    cg_ref,
    re_ref,
    rl_ref,
    gw_ref,
    o_ref,
    qbuf,
    kvbuf,
    osend,
    obuf,
    wo,
    wgu,
    wd,
    msend,
    mbuf,
    stsend,
    stbuf,
    psend,
    pbuf,
    st2send,
    st2buf,
    stream,
    sel0,
    sel1,
    outgo,
    xbuf,
    rsend,
    rbuf,
    gown,
    hbuf,
    dsend,
    dbuf,
    down_own,
    eout,
    ret,
    q_s,
    q_r,
    kv_s,
    kv_r,
    kv_f,
    o_s,
    o_r,
    wo_s,
    wo_r,
    wg_s,
    wg_r,
    wd_s,
    wd_r,
    loc,
    m_s,
    m_r,
    st_s,
    st_r,
    p_s,
    p_r,
    st2_s,
    st2_r,
    d_s,
    d_r,
    ya_s,
    ya_r,
    rx_s,
    rx_r,
    hx_s,
    hx_r,
    ry_s,
    ry_r,
    b_s,
    b_r,
):
    nz, ny, nx, t, cap = dims
    nsp = nz * 2
    ntp = ny * nx
    half = ny // KV
    grp = half * nx
    nb = nsp // grp
    cb = nsp // NCH
    rows = cb * cap
    z, c = lax.axis_index("z"), lax.axis_index("c")
    y, x = lax.axis_index("y"), lax.axis_index("x")
    s = z * 2 + c
    tp = y * nx + x
    head = y // half
    j = (y % half) * nx + x
    bf16, f32 = jnp.bfloat16, jnp.float32

    def member(g):
        return (z, c, head * half + g // nx, g % nx)

    def tp_dev(n):
        return (z, c, n // nx, n % nx)

    def sp_dev(n):
        return (n // 2, n % 2, y, x)

    barrier = pltpu.get_barrier_semaphore()
    for d in range(1, nsp):
        pl.semaphore_signal(barrier, inc=1, device_id=sp_dev((s + d) % nsp), device_id_type=MESH)
    for d in range(1, ntp):
        pl.semaphore_signal(barrier, inc=1, device_id=tp_dev((tp + d) % ntp), device_id_type=MESH)
    pl.semaphore_wait(barrier, nsp - 1 + ntp - 1)

    sends = []

    def send(src, dst, send_sem, recv_sem, device):
        copy = rcopy(src, dst, send_sem, recv_sem, device)
        copy.start()
        sends.append(copy)

    source = s % grp == j
    mine = s // grp
    order = [nz // 2]
    for d in range(nz // 2 - 1, 0, -1):
        order += [d, nz - d]

    @pl.when(source)
    def _():
        for n, d in enumerate(order):
            rcopy(
                kv_ref, kvbuf.at[mine], kv_s.at[n], kv_r.at[mine], ((z + d) % nz, mine % 2, y, x)
            ).start()
        rcopy(kv_ref, kvbuf.at[mine], kv_s.at[nz - 1], kv_r.at[mine], (z, 1 - c, y, x)).start()

    for d in range(1, grp):
        g = (j + d) % grp
        send(q_ref, qbuf.at[j], q_s.at[d], q_r.at[j], member(g))

    locals_ = []

    def local(src, dst, n):
        copy = pltpu.make_async_copy(src, dst, loc.at[n])
        copy.start()
        locals_.append(copy)

    local(wl_ref.at[pl.ds(y * nx, nx)], wo.at[y, :, 1], 0)
    local(wb_ref.at[pl.ds(ntp // 2 + y * nx, nx)], wo.at[y, :, pl.ds(2, 2)], 1)
    local(gate_ref.at[:, x], wgu.at[x, :, :, pl.ds(0, FE)], 2)
    local(up_ref.at[:, x], wgu.at[x, :, :, pl.ds(FE, FE)], 3)
    local(down_ref.at[y], wd.at[y], 4)
    for d in range(1, ny):
        to = (y + d) % ny
        dev = (z, c, to, x)
        send(
            wl_ref.at[pl.ds(to * nx, nx)], wo.at[y, :, 1], wo_s.at[0, d], wo_r.at[0, y], dev
        )
        send(
            wb_ref.at[pl.ds(ntp // 2 + to * nx, nx)],
            wo.at[y, :, pl.ds(2, 2)],
            wo_s.at[1, d],
            wo_r.at[1, y],
            dev,
        )
    for d in range(1, nx):
        to = (x + d) % nx
        dev = (z, c, y, to)
        send(gate_ref.at[:, to], wgu.at[x, :, :, pl.ds(0, FE)], wg_s.at[0, d], wg_r.at[0, x], dev)
        send(up_ref.at[:, to], wgu.at[x, :, :, pl.ds(FE, FE)], wg_s.at[1, d], wg_r.at[1, x], dev)
    for d in range(1, ny):
        to = (y + d) % ny
        send(down_ref.at[to], wd.at[y], wd_s.at[d], wd_r.at[y], (z, c, to, x))

    wo[:, :, 0] = jnp.zeros_like(wo[:, :, 0])
    qbuf[j] = q_ref[...]

    lane = lax.broadcasted_iota(jnp.int32, (t, 128), 1)
    e0 = (lane == re_ref[:, 0:1]).astype(f32)
    e1 = (lane == re_ref[:, 1:2]).astype(f32)
    before = (
        lax.broadcasted_iota(jnp.int32, (t, t), 0) > lax.broadcasted_iota(jnp.int32, (t, t), 1)
    ).astype(bf16)
    rank = dot_n(before, (e0 + e1).astype(bf16)) + (lane * cap).astype(f32)
    slot_lane = lax.broadcasted_iota(jnp.int32, (t, nsp * cap), 1)
    slot0 = jnp.sum(e0 * rank, axis=1, keepdims=True).astype(jnp.int32)
    slot1 = jnp.sum(e1 * rank, axis=1, keepdims=True).astype(jnp.int32)
    sel0[...] = (slot_lane == slot0).astype(f32).astype(bf16)
    sel1[...] = (slot_lane == slot1).astype(f32).astype(bf16)

    for i in range(nb):
        own = (mine == i) & source
        relay = (c == i % 2) & (z != (i * grp + j) // 2)

        @pl.when(own)
        def _():
            kvbuf[i] = kv_ref[...]

        @pl.when(jnp.logical_not(own))
        def _():
            landed(kvbuf.at[i], kv_r.at[i])

        @pl.when(relay)
        def _():
            rcopy(kvbuf.at[i], kvbuf.at[i], kv_f.at[i], kv_r.at[i], (z, 1 - c, y, x)).start()

    for d in range(1, grp):
        g = (j + d) % grp
        landed(qbuf.at[g], q_r.at[g])

    scale_a = HA**-0.5 * LOG2E
    scale_b = HB**-0.5 * LOG2E
    lane_a = lax.broadcasted_iota(jnp.int32, (t, 128), 1)

    def attend(scores, values, scale):
        peak = jnp.max(scores, axis=1, keepdims=True) * scale
        weights = jnp.exp2(scores * scale - peak)
        total = jnp.sum(weights, axis=1, keepdims=True)
        out = dot_n(weights.astype(bf16), values) / total
        return out, peak + jnp.log(total) * LOG2E

    def split3(v):
        a = v.astype(bf16).astype(f32)
        b = (v - a).astype(bf16).astype(f32)
        return a, b, v - a - b

    def one_head(d, carry):
        g = (j + d) % grp
        kv_l = kvbuf[:, :, 0:128].reshape(nb * t, 128)
        k_b = kvbuf[:, :, 128:256].reshape(nb * t, 128)
        v_b = kvbuf[:, :, 256:384].reshape(nb * t, 128)
        out_a, lse_a = attend(dot_t(qbuf[g, :, 0:128], kv_l), kv_l, scale_a)
        out_b, lse_b = attend(dot_t(qbuf[g, :, 128:256], k_b), v_b, scale_b)
        first = out_a
        for n, piece in enumerate(split3(lse_a) + split3(lse_b)):
            first = jnp.where(lane_a == n, piece, first)
        osend[g, :, 0:128] = first.astype(bf16)
        osend[g, :, 128:256] = out_b.astype(bf16)

        @pl.when(d < grp)
        def _():
            rcopy(osend.at[g], obuf.at[j], o_s.at[g], o_r.at[j], member(g)).start()

        @pl.when(d == grp)
        def _():
            obuf[j] = osend[g]

        return carry

    lax.fori_loop(1, grp + 1, one_head, 0)

    for d in range(1, grp):
        g = (j + d) % grp
        landed(obuf.at[g], o_r.at[g])

    lses = []
    for g in range(grp):
        stats = obuf[g, :, 0:128].astype(f32)
        lses.append(
            (
                stats[:, 0:1] + stats[:, 1:2] + stats[:, 2:3],
                stats[:, 3:4] + stats[:, 4:5] + stats[:, 5:6],
            )
        )
    top_a = functools.reduce(jnp.maximum, [v[0] for v in lses])
    top_b = functools.reduce(jnp.maximum, [v[1] for v in lses])
    sum_a, sum_b = 0.0, 0.0
    acc_a, acc_b = 0.0, 0.0
    for g in range(grp):
        wa = jnp.exp2(lses[g][0] - top_a)
        wb = jnp.exp2(lses[g][1] - top_b)
        sum_a, sum_b = sum_a + wa, sum_b + wb
        acc_a = acc_a + wa * obuf[g, :, 0:128].astype(f32)
        acc_b = acc_b + wb * obuf[g, :, 128:256].astype(f32)
    head_a = jnp.where(lane_a >= HA, acc_a / sum_a, 0.0).astype(bf16)
    head_b = (acc_b / sum_b).astype(bf16)
    msend[:, 0:128] = head_a
    msend[:, 128:256] = head_b
    for d in range(1, nx):
        to = (x + d) % nx
        send(msend, mbuf.at[x], m_s.at[d], m_r.at[x], (z, c, y, to))
    mbuf[x] = msend[...]
    row8 = lax.broadcasted_iota(jnp.int32, (8, 128), 0)
    pick_a = (row8 == 0).astype(f32)
    pick_b = (row8 == 1).astype(f32)
    sq_a, sq_b = head_a.astype(f32), head_b.astype(f32)
    last = ((1,), (1,))
    stsend[...] = jnp.zeros_like(stsend)
    stsend[:, 0:t] = dot_exact(pick_a, sq_a * sq_a, last) + dot_exact(pick_b, sq_b * sq_b, last)
    for d in range(1, ntp):
        n = (tp + d) % ntp
        send(stsend, stbuf.at[tp], st_s.at[d], st_r.at[tp], tp_dev(n))
    stbuf[tp] = stsend[...]
    for d in range(1, ntp):
        n = (tp + d) % ntp
        landed(stbuf.at[n], st_r.at[n])
    sums = jnp.sum(stbuf[...], axis=0)[:, 0:t]
    row_t = lax.broadcasted_iota(jnp.int32, (8, t), 0)
    width = jnp.where(row_t == 0, 1.0 / (ntp * HA), 1.0 / (ntp * HB))
    inverse = lax.rsqrt(sums * width + epsilon)
    first = ((0,), (0,))
    norm_a = dot_exact(inverse, pick_a, first)
    norm_b = dot_exact(inverse, pick_b, first)
    for d in range(1, nx):
        n = (x + d) % nx
        landed(mbuf.at[n], m_r.at[n])
    for copy in locals_:
        copy.wait()
    for d in range(1, ny):
        n = (y + d) % ny
        landed(wo.at[n, :, 1], wo_r.at[0, n])
        landed(wo.at[n, :, pl.ds(2, 2)], wo_r.at[1, n])
    for n in range(nx):
        gain = mg_ref[y * nx + n]
        part = mbuf[n]
        mbuf[n, :, 0:128] = (part[:, 0:128].astype(f32) * norm_a * gain[:, 0:128]).astype(bf16)
        mbuf[n, :, 128:256] = (part[:, 128:256].astype(f32) * norm_b * gain[:, 128:256]).astype(
            bf16
        )

    def project(n):
        acc = dot_n(mbuf[0], wo[n, 0].reshape(FW, FW))
        for m in range(1, nx):
            acc = acc + dot_n(mbuf[m], wo[n, m].reshape(FW, FW))
        return acc

    for d in range(1, ny):
        to = (y + d) % ny
        psend[d] = project(to).astype(bf16)
        send(psend.at[d], pbuf.at[y], p_s.at[d], p_r.at[y], (z, c, to, x))
    total = tok_ref[...].astype(f32) + project(y)
    for d in range(1, ny):
        n = (y + d) % ny
        landed(pbuf.at[n], p_r.at[n])
        total = total + pbuf[n].astype(f32)
    stream[...] = total
    ones8 = jnp.ones((8, FW), f32)
    st2send[...] = jnp.zeros_like(st2send)
    st2send[:, 0:t] = dot_exact(ones8, total * total, last)
    for d in range(1, ntp):
        n = (tp + d) % ntp
        send(st2send, st2buf.at[tp], st2_s.at[d], st2_r.at[tp], tp_dev(n))
    st2buf[tp] = st2send[...]
    for d in range(1, ntp):
        n = (tp + d) % ntp
        landed(st2buf.at[n], st2_r.at[n])
    squares = jnp.sum(st2buf[...], axis=0)[:, 0:t]
    inverse = lax.rsqrt(squares * (1.0 / (ntp * FW)) + epsilon)
    norm = dot_exact(inverse, jnp.where(row8 == 0, 1.0, 0.0), first)
    normed = (
        stream[...] * jnp.concatenate([norm, norm], axis=1) * cg_ref[...]
    ).astype(bf16)

    picked = lax.dot_general(
        sel0[...] + sel1[...], normed, (first, ((), ())), preferred_element_type=f32
    ).astype(bf16)
    for n in range(nsp):
        outgo[n] = picked[n * cap : (n + 1) * cap]
    for d in range(1, nsp):
        n = (s + d) % nsp
        send(outgo.at[n], xbuf.at[y, s], d_s.at[d], d_r.at[s], sp_dev(n))
    xbuf[y, s] = outgo[s]

    for d in range(1, nx):
        n = (x + d) % nx
        landed(wgu.at[n, :, :, pl.ds(0, FE)], wg_r.at[0, n])
        landed(wgu.at[n, :, :, pl.ds(FE, FE)], wg_r.at[1, n])
    for d in range(1, ny):
        n = (y + d) % ny
        landed(wd.at[n], wd_r.at[n])

    near = s // cb

    def chunk(k):
        return (near + k + k // 2 - 2 * (k // 3)) % NCH

    def stage_a(k):
        ch = chunk(k)
        for i in range(cb):
            b = ch * cb + i

            @pl.when(b != s)
            def _():
                landed(xbuf.at[y, b], d_r.at[b])

        part = xbuf.at[y, pl.ds(ch * cb, cb)]
        for d in range(1, ny):
            to = (y + d) % ny
            rcopy(part, part, ya_s.at[ch, d], ya_r.at[ch, y], (z, c, to, x)).start()

    def stage_b(k):
        ch = chunk(k)
        for d in range(1, ny):
            n = (y + d) % ny
            landed(xbuf.at[n, pl.ds(ch * cb, cb)], ya_r.at[ch, n])
        xs = [xbuf[n, pl.ds(ch * cb, cb)].reshape(rows, FW) for n in range(ny)]

        def expand(n):
            acc = dot_n(xs[0], wgu[n, 0])
            for m in range(1, ny):
                acc = acc + dot_n(xs[m], wgu[n, m])
            return acc

        for d in range(1, nx):
            to = (x + d) % nx
            rsend[ch, d] = expand(to).astype(bf16)
            rcopy(
                rsend.at[ch, d], rbuf.at[ch, x], rx_s.at[ch, d], rx_r.at[ch, x], (z, c, y, to)
            ).start()
        gown[ch] = expand(x)

    def stage_c(k):
        ch = chunk(k)
        both = gown[ch]
        for d in range(1, nx):
            n = (x + d) % nx
            landed(rbuf.at[ch, n], rx_r.at[ch, n])
            both = both + rbuf[ch, n].astype(f32)
        gate_value = both[:, 0:FE]
        hidden = (gate_value / (1.0 + jnp.exp(-gate_value)) * both[:, FE:]).astype(bf16)
        hbuf[ch, x] = hidden
        for d in range(1, nx):
            to = (x + d) % nx
            rcopy(
                hbuf.at[ch, x], hbuf.at[ch, x], hx_s.at[ch, d], hx_r.at[ch, x], (z, c, y, to)
            ).start()

    def stage_d(k):
        ch = chunk(k)
        for d in range(1, nx):
            n = (x + d) % nx
            landed(hbuf.at[ch, n], hx_r.at[ch, n])
        wide = jnp.concatenate([hbuf[ch, n] for n in range(nx)], axis=1)
        for d in range(1, ny):
            to = (y + d) % ny
            dsend[ch, d] = dot_n(wide, wd[to]).astype(bf16)
            rcopy(
                dsend.at[ch, d], dbuf.at[ch, y], ry_s.at[ch, d], ry_r.at[ch, y], (z, c, to, x)
            ).start()
        down_own[ch] = dot_n(wide, wd[y])

    def stage_e(k):
        ch = chunk(k)
        acc = down_own[ch]
        for d in range(1, ny):
            n = (y + d) % ny
            landed(dbuf.at[ch, n], ry_r.at[ch, n])
            acc = acc + dbuf[ch, n].astype(f32)
        eout[pl.ds(ch * cb, cb)] = acc.astype(bf16).reshape(cb, cap, FW)
        for i in range(cb):
            b = ch * cb + i

            @pl.when(b != s)
            def _():
                rcopy(eout.at[b], ret.at[s], b_s.at[b], b_r.at[s], sp_dev(b)).start()

            @pl.when(b == s)
            def _():
                ret[s] = eout[b]

    stages = (stage_a, stage_b, stage_c, stage_d, stage_e)

    def step(i, carry):
        for lag, stage in enumerate(stages):

            @pl.when((i >= lag) & (i < NCH + lag))
            def _():
                stage(i - lag)

        return carry

    lax.fori_loop(0, NCH + len(stages) - 1, step, 0)

    for d in range(1, nsp):
        n = (s + d) % nsp
        landed(ret.at[n], b_r.at[n])
    back = ret[...].reshape(nsp * cap, FW)
    gap = rl_ref[:, 0:1] - rl_ref[:, 1:2]
    w0 = gw_ref[...] / (1.0 + jnp.exp(-gap))
    w1 = gw_ref[...] / (1.0 + jnp.exp(gap))
    routed = w0 * dot_n(sel0[...], back) + w1 * dot_n(sel1[...], back)
    o_ref[...] = (stream[...] + routed).astype(bf16)

    for copy in sends:
        copy.wait_send()

    @pl.when(source)
    def _():
        for n in range(nz):
            landed(kv_ref, kv_s.at[n])

    for i in range(nb):
        relay = (c == i % 2) & (z != (i * grp + j) // 2)

        @pl.when(relay)
        def _():
            landed(kvbuf.at[i], kv_f.at[i])

    for d in range(1, grp):
        g = (j + d) % grp
        landed(osend.at[g], o_s.at[g])
    for ch in range(NCH):
        for d in range(1, ny):
            landed(xbuf.at[y, pl.ds(ch * cb, cb)], ya_s.at[ch, d])
            landed(dsend.at[ch, d], ry_s.at[ch, d])
        for d in range(1, nx):
            landed(rsend.at[ch, d], rx_s.at[ch, d])
            landed(hbuf.at[ch, x], hx_s.at[ch, d])
    for d in range(1, nsp):
        b = (s + d) % nsp
        landed(eout.at[b], b_s.at[b])


def on_device(
    tokens,
    lean_query,
    lean_key,
    lean_value,
    lean_gains,
    broad_query,
    broad_key,
    broad_value,
    broad_gains,
    mixer_gain,
    output_weight,
    channel_gain,
    gate_weight,
    up_weight,
    down_weight,
    route_experts,
    route_logits,
    group_weight,
):
    nz, ny, nx = lax.axis_size("z"), lax.axis_size("y"), lax.axis_size("x")
    nsp, ntp = nz * 2, ny * nx
    t = tokens.shape[0]
    cap = t // (nsp // GROUPS)
    half = ny // KV
    grp = half * nx
    nb = nsp // grp
    cb = nsp // NCH
    rows = cb * cap
    bf16, f32 = jnp.bfloat16, jnp.float32
    s = lax.axis_index("z") * 2 + lax.axis_index("c")
    head = lax.axis_index("y") // half
    positions = s * t + jnp.arange(t, dtype=jnp.int32)

    def own(array):
        return lax.dynamic_index_in_dim(array, head, 1, keepdims=False)

    q_all = jnp.concatenate(
        [
            prepare(lean_query[:, 0], lean_gains[0], positions),
            jnp.zeros((t, HA), bf16),
            prepare(broad_query[:, 0], broad_gains[0], positions),
        ],
        axis=1,
    )
    kv_all = jnp.concatenate(
        [
            prepare(own(lean_key), lean_gains[1], positions),
            own(lean_value),
            prepare(own(broad_key), broad_gains[1], positions),
            own(broad_value),
        ],
        axis=1,
    )
    gains = jnp.concatenate(
        [
            jnp.zeros((ntp, HA), f32),
            mixer_gain[: ntp * HA].reshape(ntp, HA),
            mixer_gain[ntp * HA :].reshape(ntp, HB),
        ],
        axis=1,
    ).reshape(ntp, 1, FW)
    vm = pl.BlockSpec(memory_space=pltpu.VMEM)
    hbm = pl.BlockSpec(memory_space=pl.ANY)
    dma = pltpu.SemaphoreType.DMA
    return pl.pallas_call(
        functools.partial(layer_kernel, (nz, ny, nx, t, cap)),
        out_shape=jax.ShapeDtypeStruct((t, FW), bf16),
        in_specs=[vm, vm, vm, hbm, hbm, hbm, hbm, hbm, vm, vm, vm, vm, vm],
        out_specs=vm,
        scratch_shapes=[
            pltpu.VMEM((grp, t, 256), bf16),
            pltpu.VMEM((nb, t, 384), bf16),
            pltpu.VMEM((grp, t, 256), bf16),
            pltpu.VMEM((grp, t, 256), bf16),
            pltpu.VMEM((ny, nx, 4, 64, FW), bf16),
            pltpu.VMEM((nx, ny, FW, FW), bf16),
            pltpu.VMEM((ny, nx * FE, FW), bf16),
            pltpu.VMEM((t, 256), bf16),
            pltpu.VMEM((nx, t, 256), bf16),
            pltpu.VMEM((8, 256), f32),
            pltpu.VMEM((ntp, 8, 256), f32),
            pltpu.VMEM((ny, t, FW), bf16),
            pltpu.VMEM((ny, t, FW), bf16),
            pltpu.VMEM((8, 256), f32),
            pltpu.VMEM((ntp, 8, 256), f32),
            pltpu.VMEM((t, FW), f32),
            pltpu.VMEM((t, nsp * cap), bf16),
            pltpu.VMEM((t, nsp * cap), bf16),
            pltpu.VMEM((nsp, cap, FW), bf16),
            pltpu.VMEM((ny, nsp, cap, FW), bf16),
            pltpu.VMEM((NCH, nx, rows, FW), bf16),
            pltpu.VMEM((NCH, nx, rows, FW), bf16),
            pltpu.VMEM((NCH, rows, FW), f32),
            pltpu.VMEM((NCH, nx, rows, FE), bf16),
            pltpu.VMEM((NCH, ny, rows, FW), bf16),
            pltpu.VMEM((NCH, ny, rows, FW), bf16),
            pltpu.VMEM((NCH, rows, FW), f32),
            pltpu.VMEM((nsp, cap, FW), bf16),
            pltpu.VMEM((nsp, cap, FW), bf16),
            dma((grp,)),
            dma((grp,)),
            dma((nz,)),
            dma((nb,)),
            dma((nb,)),
            dma((grp,)),
            dma((grp,)),
            dma((2, ny)),
            dma((2, ny)),
            dma((2, nx)),
            dma((2, nx)),
            dma((ny,)),
            dma((ny,)),
            dma((5,)),
            dma((nx,)),
            dma((nx,)),
            dma((ntp,)),
            dma((ntp,)),
            dma((ny,)),
            dma((ny,)),
            dma((ntp,)),
            dma((ntp,)),
            dma((nsp,)),
            dma((nsp,)),
            dma((NCH, ny)),
            dma((NCH, ny)),
            dma((NCH, nx)),
            dma((NCH, nx)),
            dma((NCH, nx)),
            dma((NCH, nx)),
            dma((NCH, ny)),
            dma((NCH, ny)),
            dma((nsp,)),
            dma((nsp,)),
        ],
        compiler_params=pltpu.CompilerParams(
            collective_id=0, has_side_effects=True, vmem_limit_bytes=60 * 1024 * 1024
        ),
    )(
        q_all,
        kv_all,
        tokens,
        output_weight.reshape(3 * ntp, 64, FW),
        output_weight.reshape(3 * ntp // 2, 2, 64, FW),
        gate_weight.reshape(ny, nx, FW, FE),
        up_weight.reshape(ny, nx, FW, FE),
        down_weight.reshape(ny, nx * FE, FW),
        gains,
        channel_gain.reshape(1, FW),
        route_experts,
        route_logits,
        group_weight.reshape(t, 1),
    )


def solution(mesh):
    finer = Mesh(
        mesh.devices.reshape(mesh.shape["sp"] // 2, 2, NY, NX), ("z", "c", "y", "x")
    )
    sp, tp = ("z", "c"), ("y", "x")
    return jax.shard_map(
        on_device,
        mesh=finer,
        in_specs=(
            P(sp, tp),
            P(sp, tp, None),
            P(sp, None, None),
            P(sp, None, None),
            P(),
            P(sp, tp, None),
            P(sp, None, None),
            P(sp, None, None),
            P(),
            P(),
            P(None, tp),
            P(tp),
            P(sp, None, tp),
            P(sp, None, tp),
            P(sp, None, tp),
            P(sp, None),
            P(sp, None),
            P(sp),
        ),
        out_specs=P(sp, tp),
        check_vma=False,
    )
```

time: 402 us -> 177 us (0.44)
  waiting for transfers between devices: 225 us -> 0 us
  Pallas kernels: 0 us -> 161 us
  blocking collectives: 102 us -> 0 us
  matrix products: 18.3 us -> 0 us
  starting transfers between devices: 17.2 us -> 0 us
  between operations: 13.6 us -> 0.26 us
  local copies, waits for them, and re-layouts: 16.8 us -> 8.56 us
  other arithmetic: 8.63 us -> 4.26 us
    all_gather x3 -> x0, waiting for transfers between devices: 191 us -> none  [the longest x1 73.3 us: sent_together(): lax.all_gather(both, axis, axis=dim, tiled=True)]
    pallas_call x0 -> x1, Pallas kernels: none -> 161 us  [on_device(): pl.pallas_call(functools.partial(layer_kernel, (nz, ny, nx, t, cap)), out...]
    all_gather x3 -> x0, blocking collectives: 53.7 us -> none  [the longest x1 19.2 us: on_device(): lax.all_gather(finish_heads(broad_state), TP, axis=1, tiled=True)]
    all_to_all x1 -> x0, blocking collectives: 48.3 us -> none  [on_device(): lax.all_to_all(outgoing, 'sp', split_axis=0, concat_axis=0, tiled=True)]
    all_to_all x2 -> x0, waiting for transfers between devices: 33.7 us -> none  [the longest x1 27.6 us: on_device(): lax.all_to_all(result, 'sp', split_axis=0, concat_axis=0, tiled=True)]
    dot_general x9 -> x0, matrix products: 18.3 us -> none  [the longest x1 4.72 us: on_device(): jnp.dot(flat_rows, gate_part, preferred_element_type=jnp.float32)]
    all_to_all x2 -> x0, starting transfers between devices: 16.9 us -> none  [the longest x1 13.2 us: on_device(): lax.all_to_all(result, 'sp', split_axis=0, concat_axis=0, tiled=True)]
    gather x2 -> x0, local copies, waits for them, and re-layouts: 4.7 us -> none  [the longest x1 2.66 us: on_device(): normed[source]]
  transfers between devices with their start and end apart: 5 -> 0, of which waited for: 5 -> 0; matrix products, arithmetic and copies ran while one was open for 2% -> 0% of each run, Pallas kernels for 0% -> 0%
where the time goes in v1:
time: 177 us; the launch traced here: 174 us
  Pallas kernels  161 us (91%)
  local copies, waits for them, and re-layouts  8.56 us (5%)
  other arithmetic  4.26 us (2%)
    pallas_call x1, Pallas kernels, on_device(): pl.pallas_call(functools.partial(layer_kernel, (nz, ny, nx, t, cap)), out...  161 us

profile of v1, /device:TPU:1, one launch (start us, length us, event | category | flops | bytes accessed | tf_op | source)
XLA Modules:
  0.0 173.6 jit_solution(7769750976739660532)
XLA Ops:
  0.0 0.0 copy-start
  0.0 0.0 copy-start.1
  0.0 0.0 copy-start.7
  0.0 1.2 constant_dynamic-slice_fusion
  1.2 0.1 fusion.38
  1.3 0.8 slice_bitcast_fusion.1
  2.1 0.1 fusion.39
  2.2 0.9 fusion.34
  3.1 0.9 fusion.35
  4.1 0.0 copy-start.3
  4.1 0.9 fusion.67
  5.0 0.0 copy-done
  5.0 0.1 copy.45
  5.1 0.1 fusion.36
  5.2 0.0 copy-done.1
  5.2 0.0 copy-start.4
  5.3 0.1 copy.33
  5.4 0.1 fusion.32
  5.5 0.0 copy-done.7
  5.5 0.0 copy-start.5
  5.5 0.0 copy-start.6
  5.6 0.1 fusion.33
  5.7 0.0 slice-start
  5.7 0.0 copy-start.2
  5.7 0.9 fusion.51
  6.6 0.0 copy-done.3
  6.7 0.1 copy.39
  6.8 0.8 concatenate.20.kv_ref
  7.6 0.8 concatenate.19.q_ref
  8.5 0.0 copy-done.4
  8.5 0.8 copy.42.re_ref
  9.2 0.0 copy-done.5
  9.2 0.8 copy.43.rl_ref
  10.0 0.0 copy-done.6
  10.0 0.8 copy.44.gw_ref
  10.8 0.0 slice-done
  10.8 0.1 reshape.135
  10.8 0.0 copy-done.2
  10.8 0.1 pad_maximum_fusion
  10.9 0.6 reshape.136.mg_ref
  11.5 160.5 %shard_map.172 = bf16[192,256]{1,0:T(8,128)(2,1)} custom-call(bf16[192,256]{1,0:T(8,128)(2,1)} %concatenate.19.q_ref, bf16[192,384]{1,0:T(8,128)(2,1)} %concatenate.20.kv_ref, bf16[192,256]{1,0:T(8,128)(2,1)} %tok_ref.1, bf16[48,64,256]{2,1,0:T(8,128)(2,1)} %bitcast.40, bf16[24,2,64,256]{3,2,1,0:T(8,128)(2,1)} %bitcast.41, ...), custom_call_target="tpu_custom_call" | custom-call | tf_op jit(solution)/shard_map/pallas_call | solution.py:672
  172.0 1.5 copy.56
  (15 shorter events, 0.1 us)
Async XLA Ops:
  0.0 5.0 %copy-start = (bf16[192,2,64]{0,2,1:T(8,128)(2,1)S(1)}, bf16[192,2,64]{0,2,1:T(8,128)(2,1)}, u32[]{:S(2)}) copy-start(bf16[192,2,64]{0,2,1:T(8,128)(2,1)} %param.20) | copy-start | bytes 147460
  0.0 5.2 %copy-start.1 = (bf16[192,1,64]{0,2,1:T(8,128)(2,1)S(1)}, bf16[192,1,64]{0,2,1:T(8,128)(2,1)}, u32[]{:S(2)}) copy-start(bf16[192,1,64]{0,2,1:T(8,128)(2,1)} %param.19) | copy-start | bytes 73732
  0.0 5.5 %copy-start.7 = (f32[2,64]{1,0:T(2,128)S(1)}, f32[2,64]{1,0:T(2,128)}, u32[]{:S(2)}) copy-start(f32[2,64]{1,0:T(2,128)} %param.22) | copy-start | bytes 1540
  4.1 2.6 %copy-start.3 = (bf16[192,2,64]{0,2,1:T(8,128)(2,1)S(1)}, bf16[192,2,64]{0,2,1:T(8,128)(2,1)}, u32[]{:S(2)}) copy-start(bf16[192,2,64]{0,2,1:T(8,128)(2,1)} %param.21) | copy-start | bytes 147460
  5.2 3.2 %copy-start.4 = (s32[192,2]{0,1:T(2,128)S(1)}, s32[192,2]{0,1:T(2,128)}, u32[]{:S(2)}) copy-start(s32[192,2]{0,1:T(2,128)} %param.33) | copy-start | bytes 4612
  5.5 3.7 %copy-start.5 = (f32[192,2]{0,1:T(2,128)S(1)}, f32[192,2]{0,1:T(2,128)}, u32[]{:S(2)}) copy-start(f32[192,2]{0,1:T(2,128)} %param.34) | copy-start | bytes 4612
  5.5 4.5 %copy-start.6 = (f32[192]{0:T(256)S(1)}, f32[192]{0:T(256)}, u32[]{:S(2)}) copy-start(f32[192]{0:T(256)} %param.35) | copy-start | bytes 2308
  5.7 5.1 %slice-start = ((f32[3072]{0:T(1024)}), f32[1024]{0:T(1024)S(1)}, s32[]{:S(2)}) async-start(f32[3072]{0:T(1024)} %param.27), calls=%async_computation | async-start | bytes 8192 | tf_op jit(solution)/shard_map/slice | solution.py:664
  5.7 5.1 %copy-start.2 = (f32[3072]{0:T(1024)S(1)}, f32[3072]{0:T(1024)}, u32[]{:S(2)}) copy-start(f32[3072]{0:T(1024)} %param.27) | copy-start | bytes 36868

commit v2 on v1

--- a/solution.py
+++ b/solution.py
@@ -11,6 +11,7 @@
 
 D = 4096
 GRID_W = 64
+GRID_BITS = 6
 KV = 2
 GROUPS = 4
 NY, NX = 4, 4
@@ -24,43 +25,6 @@
 LOG2E = 1.4426950408889634
 
 
-def axial_angles(positions, head_size):
-    quarter = head_size // 4
-    frequency = theta_base ** (-jnp.arange(quarter, dtype=jnp.float32) / quarter)
-    grid_rows = (positions // GRID_W).astype(jnp.float32)
-    grid_columns = (positions % GRID_W).astype(jnp.float32)
-    return (grid_rows[:, None] * frequency[None, :], grid_columns[:, None] * frequency[None, :])
-
-
-def turn_half(values, angles):
-    half_width = values.shape[-1] // 2
-    first_half = values[..., :half_width]
-    second = values[..., half_width:]
-    cosine = jnp.cos(angles)
-    sine_part = jnp.sin(angles)
-    return jnp.concatenate(
-        [first_half * cosine - second * sine_part, second * cosine + first_half * sine_part],
-        axis=-1,
-    )
-
-
-def prepare(raw_values, gain_row, positions):
-    values = raw_values.astype(jnp.float32)
-    values = (
-        values * lax.rsqrt(jnp.mean(values * values, axis=-1, keepdims=True) + epsilon) * gain_row
-    )
-    row_angles, column_angles = axial_angles(positions, raw_values.shape[-1])
-    half_width = raw_values.shape[-1] // 2
-    turned = jnp.concatenate(
-        [
-            turn_half(values[..., :half_width], row_angles),
-            turn_half(values[..., half_width:], column_angles),
-        ],
-        axis=-1,
-    )
-    return turned.astype(jnp.bfloat16)
-
-
 def rcopy(src, dst, send_sem, recv_sem, device):
     return pltpu.make_async_remote_copy(
         src_ref=src,
@@ -96,8 +60,14 @@
 
 def layer_kernel(
     dims,
-    q_ref,
-    kv_ref,
+    lq_ref,
+    lk_ref,
+    lv_ref,
+    lg_ref,
+    bq_ref,
+    bk_ref,
+    bv_ref,
+    bg_ref,
     tok_ref,
     wl_ref,
     wb_ref,
@@ -110,8 +80,12 @@
     rl_ref,
     gw_ref,
     o_ref,
+    q_ref,
+    kvl_ref,
+    kvb_ref,
     qbuf,
-    kvbuf,
+    kvl,
+    kvb,
     osend,
     obuf,
     wo,
@@ -204,6 +178,80 @@
         pl.semaphore_signal(barrier, inc=1, device_id=sp_dev((s + d) % nsp), device_id_type=MESH)
     for d in range(1, ntp):
         pl.semaphore_signal(barrier, inc=1, device_id=tp_dev((tp + d) % ntp), device_id_type=MESH)
+
+    def turned(raw, swapped, gain, size):
+        quarter = size // 4
+        lane = lax.broadcasted_iota(jnp.int32, (t, 128), 1)
+        at = lax.broadcasted_iota(jnp.int32, (t, 128), 0) + s * t
+        spot = jnp.where(lane < size // 2, at >> GRID_BITS, at & (GRID_W - 1)).astype(f32)
+        step = (lane & (quarter - 1)).astype(f32) * (-math.log(theta_base) / quarter)
+        angle = spot * jnp.exp(step)
+        cosine = jnp.cos(angle)
+        sine = jnp.where((lane & quarter) == 0, -1.0, 1.0) * jnp.sin(angle)
+        results = []
+        for (a, b), (g, h) in zip(zip(raw, swapped), gain):
+            scale = lax.rsqrt(jnp.sum(a * a, axis=1, keepdims=True) * (1.0 / size) + epsilon)
+            results.append(scale * (a * (g * cosine) + b * (h * sine)))
+        return results
+
+    def unit(size, shift):
+        row = lax.broadcasted_iota(jnp.int32, (size, 128), 0)
+        lane = lax.broadcasted_iota(jnp.int32, (size, 128), 1)
+        return row + shift == lane, row == (lane ^ (size // 4))
+
+    def gain_pair(ref, swap):
+        pairs = dot_exact(ref[...], swap, ((1,), (0,)))
+        return pairs[0:1], pairs[1:2]
+
+    first = ((0,), (0,))
+
+    def flipped(array, matrix):
+        return lax.dot_general(array, matrix, (first, ((), ())), preferred_element_type=f32)
+
+    same, swap = unit(HA, 0)
+    place, _ = unit(HA, HA)
+    same_b, swap_b, place_b = same.astype(bf16), swap.astype(bf16), place.astype(bf16)
+    lk = lk_ref[head]
+    g_raw, g_swap = gain_pair(lg_ref, same.astype(f32)), gain_pair(lg_ref, swap.astype(f32))
+    q_a, k_a = turned(
+        (flipped(lq_ref[...], same_b), flipped(lk, same_b)),
+        (flipped(lq_ref[...], swap_b), flipped(lk, swap_b)),
+        tuple(zip(g_raw, g_swap)),
+        HA,
+    )
+    q_ref[:, 0:128] = q_a.astype(bf16)
+    kvl_ref[...] = (k_a + flipped(lv_ref[head], place_b)).astype(bf16)
+    _, swap = unit(HB, 0)
+    swap_b = swap.astype(bf16)
+    pair_row = lax.broadcasted_iota(jnp.int32, (t, KV * t), 0) * KV + head
+    pick = (pair_row == lax.broadcasted_iota(jnp.int32, (t, KV * t), 1)).astype(bf16)
+    k_raw = dot_n(pick, bk_ref[...])
+    g_raw = (bg_ref[0:1], bg_ref[1:2])
+    q_b, k_b = turned(
+        (bq_ref[...].astype(f32), k_raw),
+        (dot_n(bq_ref[...], swap_b), dot_n(k_raw.astype(bf16), swap_b)),
+        tuple(zip(g_raw, gain_pair(bg_ref, swap.astype(f32)))),
+        HB,
+    )
+    q_ref[:, 128:256] = q_b.astype(bf16)
+    kvb_ref[:, 0:128] = k_b.astype(bf16)
+    kvb_ref[:, 128:256] = dot_n(pick, bv_ref[...]).astype(bf16)
+
+    experts = lax.broadcasted_iota(jnp.int32, (nsp, t), 0)
+    e0 = (experts == re_ref[0:1]).astype(f32)
+    e1 = (experts == re_ref[1:2]).astype(f32)
+    before = (
+        lax.broadcasted_iota(jnp.int32, (t, t), 0) < lax.broadcasted_iota(jnp.int32, (t, t), 1)
+    ).astype(bf16)
+    rank = dot_n((e0 + e1).astype(bf16), before) + (experts * cap).astype(f32)
+    slot_row = lax.broadcasted_iota(jnp.int32, (nsp * cap, t), 0)
+    slot0 = jnp.sum(e0 * rank, axis=0, keepdims=True).astype(jnp.int32)
+    slot1 = jnp.sum(e1 * rank, axis=0, keepdims=True).astype(jnp.int32)
+    sel0[...] = (slot_row == slot0).astype(f32).astype(bf16)
+    sel1[...] = (slot_row == slot1).astype(f32).astype(bf16)
+    wo[:, :, 0] = jnp.zeros_like(wo[:, :, 0])
+    qbuf[j] = q_ref[...]
+
     pl.semaphore_wait(barrier, nsp - 1 + ntp - 1)
 
     sends = []
@@ -218,14 +266,22 @@
     order = [nz // 2]
     for d in range(nz // 2 - 1, 0, -1):
         order += [d, nz - d]
+    kv_pairs = ((kvl_ref, kvl), (kvb_ref, kvb))
 
     @pl.when(source)
     def _():
-        for n, d in enumerate(order):
+        for part, (src, dst) in enumerate(kv_pairs):
+            for n, d in enumerate(order):
+                rcopy(
+                    src,
+                    dst.at[mine],
+                    kv_s.at[part, n],
+                    kv_r.at[part, mine],
+                    ((z + d) % nz, mine % 2, y, x),
+                ).start()
             rcopy(
-                kv_ref, kvbuf.at[mine], kv_s.at[n], kv_r.at[mine], ((z + d) % nz, mine % 2, y, x)
+                src, dst.at[mine], kv_s.at[part, nz - 1], kv_r.at[part, mine], (z, 1 - c, y, x)
             ).start()
-        rcopy(kv_ref, kvbuf.at[mine], kv_s.at[nz - 1], kv_r.at[mine], (z, 1 - c, y, x)).start()
 
     for d in range(1, grp):
         g = (j + d) % grp
@@ -241,14 +297,10 @@
     local(wl_ref.at[pl.ds(y * nx, nx)], wo.at[y, :, 1], 0)
     local(wb_ref.at[pl.ds(ntp // 2 + y * nx, nx)], wo.at[y, :, pl.ds(2, 2)], 1)
     local(gate_ref.at[:, x], wgu.at[x, :, :, pl.ds(0, FE)], 2)
-    local(up_ref.at[:, x], wgu.at[x, :, :, pl.ds(FE, FE)], 3)
-    local(down_ref.at[y], wd.at[y], 4)
     for d in range(1, ny):
         to = (y + d) % ny
         dev = (z, c, to, x)
-        send(
-            wl_ref.at[pl.ds(to * nx, nx)], wo.at[y, :, 1], wo_s.at[0, d], wo_r.at[0, y], dev
-        )
+        send(wl_ref.at[pl.ds(to * nx, nx)], wo.at[y, :, 1], wo_s.at[0, d], wo_r.at[0, y], dev)
         send(
             wb_ref.at[pl.ds(ntp // 2 + to * nx, nx)],
             wo.at[y, :, pl.ds(2, 2)],
@@ -260,43 +312,42 @@
         to = (x + d) % nx
         dev = (z, c, y, to)
         send(gate_ref.at[:, to], wgu.at[x, :, :, pl.ds(0, FE)], wg_s.at[0, d], wg_r.at[0, x], dev)
-        send(up_ref.at[:, to], wgu.at[x, :, :, pl.ds(FE, FE)], wg_s.at[1, d], wg_r.at[1, x], dev)
-    for d in range(1, ny):
-        to = (y + d) % ny
-        send(down_ref.at[to], wd.at[y], wd_s.at[d], wd_r.at[y], (z, c, to, x))
-
-    wo[:, :, 0] = jnp.zeros_like(wo[:, :, 0])
-    qbuf[j] = q_ref[...]
-
-    lane = lax.broadcasted_iota(jnp.int32, (t, 128), 1)
-    e0 = (lane == re_ref[:, 0:1]).astype(f32)
-    e1 = (lane == re_ref[:, 1:2]).astype(f32)
-    before = (
-        lax.broadcasted_iota(jnp.int32, (t, t), 0) > lax.broadcasted_iota(jnp.int32, (t, t), 1)
-    ).astype(bf16)
-    rank = dot_n(before, (e0 + e1).astype(bf16)) + (lane * cap).astype(f32)
-    slot_lane = lax.broadcasted_iota(jnp.int32, (t, nsp * cap), 1)
-    slot0 = jnp.sum(e0 * rank, axis=1, keepdims=True).astype(jnp.int32)
-    slot1 = jnp.sum(e1 * rank, axis=1, keepdims=True).astype(jnp.int32)
-    sel0[...] = (slot_lane == slot0).astype(f32).astype(bf16)
-    sel1[...] = (slot_lane == slot1).astype(f32).astype(bf16)
-
-    for i in range(nb):
-        own = (mine == i) & source
-        relay = (c == i % 2) & (z != (i * grp + j) // 2)
-
-        @pl.when(own)
-        def _():
-            kvbuf[i] = kv_ref[...]
-
-        @pl.when(jnp.logical_not(own))
-        def _():
-            landed(kvbuf.at[i], kv_r.at[i])
-
-        @pl.when(relay)
-        def _():
-            rcopy(kvbuf.at[i], kvbuf.at[i], kv_f.at[i], kv_r.at[i], (z, 1 - c, y, x)).start()
-
+
+    def later_weights():
+        for d in range(1, nx):
+            to = (x + d) % nx
+            dev = (z, c, y, to)
+            send(
+                up_ref.at[:, to], wgu.at[x, :, :, pl.ds(FE, FE)], wg_s.at[1, d], wg_r.at[1, x], dev
+            )
+        for d in range(1, ny):
+            to = (y + d) % ny
+            send(down_ref.at[to], wd.at[y], wd_s.at[d], wd_r.at[y], (z, c, to, x))
+
+    local(up_ref.at[:, x], wgu.at[x, :, :, pl.ds(FE, FE)], 3)
+    local(down_ref.at[y], wd.at[y], 4)
+
+    def arrive(part):
+        src, dst = kv_pairs[part]
+        for i in range(nb):
+            own = (mine == i) & source
+            relay = (c == i % 2) & (z != (i * grp + j) // 2)
+
+            @pl.when(own)
+            def _():
+                dst[i] = src[...]
+
+            @pl.when(jnp.logical_not(own))
+            def _():
+                landed(dst.at[i], kv_r.at[part, i])
+
+            @pl.when(relay)
+            def _():
+                rcopy(
+                    dst.at[i], dst.at[i], kv_f.at[part, i], kv_r.at[part, i], (z, 1 - c, y, x)
+                ).start()
+
+    arrive(0)
     for d in range(1, grp):
         g = (j + d) % grp
         landed(qbuf.at[g], q_r.at[g])
@@ -317,18 +368,24 @@
         b = (v - a).astype(bf16).astype(f32)
         return a, b, v - a - b
 
-    def one_head(d, carry):
+    def marked(value, lse, at):
+        for n, piece in enumerate(split3(lse)):
+            value = jnp.where(lane_a == at + n, piece, value)
+        return value
+
+    def lean_head(g, carry):
+        kv_l = kvl[...].reshape(nb * t, 128)
+        out, lse = attend(dot_t(qbuf[g, :, 0:128], kv_l), kv_l, scale_a)
+        osend[g, :, 0:128] = marked(out, lse, 0).astype(bf16)
+        return carry
+
+    def broad_head(d, carry):
         g = (j + d) % grp
-        kv_l = kvbuf[:, :, 0:128].reshape(nb * t, 128)
-        k_b = kvbuf[:, :, 128:256].reshape(nb * t, 128)
-        v_b = kvbuf[:, :, 256:384].reshape(nb * t, 128)
-        out_a, lse_a = attend(dot_t(qbuf[g, :, 0:128], kv_l), kv_l, scale_a)
-        out_b, lse_b = attend(dot_t(qbuf[g, :, 128:256], k_b), v_b, scale_b)
-        first = out_a
-        for n, piece in enumerate(split3(lse_a) + split3(lse_b)):
-            first = jnp.where(lane_a == n, piece, first)
-        osend[g, :, 0:128] = first.astype(bf16)
-        osend[g, :, 128:256] = out_b.astype(bf16)
+        k_b = kvb[:, :, 0:128].reshape(nb * t, 128)
+        v_b = kvb[:, :, 128:256].reshape(nb * t, 128)
+        out, lse = attend(dot_t(qbuf[g, :, 128:256], k_b), v_b, scale_b)
+        osend[g, :, 0:128] = marked(osend[g, :, 0:128].astype(f32), lse, 3).astype(bf16)
+        osend[g, :, 128:256] = out.astype(bf16)
 
         @pl.when(d < grp)
         def _():
@@ -340,7 +397,9 @@
 
         return carry
 
-    lax.fori_loop(1, grp + 1, one_head, 0)
+    lax.fori_loop(0, grp, lean_head, 0)
+    arrive(1)
+    lax.fori_loop(1, grp + 1, broad_head, 0)
 
     for d in range(1, grp):
         g = (j + d) % grp
@@ -369,10 +428,6 @@
     head_b = (acc_b / sum_b).astype(bf16)
     msend[:, 0:128] = head_a
     msend[:, 128:256] = head_b
-    for d in range(1, nx):
-        to = (x + d) % nx
-        send(msend, mbuf.at[x], m_s.at[d], m_r.at[x], (z, c, y, to))
-    mbuf[x] = msend[...]
     row8 = lax.broadcasted_iota(jnp.int32, (8, 128), 0)
     pick_a = (row8 == 0).astype(f32)
     pick_b = (row8 == 1).astype(f32)
@@ -384,6 +439,10 @@
         n = (tp + d) % ntp
         send(stsend, stbuf.at[tp], st_s.at[d], st_r.at[tp], tp_dev(n))
     stbuf[tp] = stsend[...]
+    for d in range(1, nx):
+        to = (x + d) % nx
+        send(msend, mbuf.at[x], m_s.at[d], m_r.at[x], (z, c, y, to))
+    mbuf[x] = msend[...]
     for d in range(1, ntp):
         n = (tp + d) % ntp
         landed(stbuf.at[n], st_r.at[n])
@@ -391,7 +450,6 @@
     row_t = lax.broadcasted_iota(jnp.int32, (8, t), 0)
     width = jnp.where(row_t == 0, 1.0 / (ntp * HA), 1.0 / (ntp * HB))
     inverse = lax.rsqrt(sums * width + epsilon)
-    first = ((0,), (0,))
     norm_a = dot_exact(inverse, pick_a, first)
     norm_b = dot_exact(inverse, pick_b, first)
     for d in range(1, nx):
@@ -404,12 +462,13 @@
         landed(wo.at[n, :, 1], wo_r.at[0, n])
         landed(wo.at[n, :, pl.ds(2, 2)], wo_r.at[1, n])
     for n in range(nx):
-        gain = mg_ref[y * nx + n]
+        gain = mg_ref[pl.ds((y * nx + n) // 2, 1)]
+        if n % 2 == 0:
+            gain = pltpu.roll(gain, HA, 1)
         part = mbuf[n]
-        mbuf[n, :, 0:128] = (part[:, 0:128].astype(f32) * norm_a * gain[:, 0:128]).astype(bf16)
-        mbuf[n, :, 128:256] = (part[:, 128:256].astype(f32) * norm_b * gain[:, 128:256]).astype(
-            bf16
-        )
+        mbuf[n, :, 0:128] = (part[:, 0:128].astype(f32) * norm_a * gain).astype(bf16)
+        gain = mg_ref[pl.ds(ntp // 2 + y * nx + n, 1)]
+        mbuf[n, :, 128:256] = (part[:, 128:256].astype(f32) * norm_b * gain).astype(bf16)
 
     def project(n):
         acc = dot_n(mbuf[0], wo[n, 0].reshape(FW, FW))
@@ -444,15 +503,24 @@
         stream[...] * jnp.concatenate([norm, norm], axis=1) * cg_ref[...]
     ).astype(bf16)
 
-    picked = lax.dot_general(
-        sel0[...] + sel1[...], normed, (first, ((), ())), preferred_element_type=f32
-    ).astype(bf16)
+    picked = dot_n(sel0[...] + sel1[...], normed).astype(bf16)
     for n in range(nsp):
         outgo[n] = picked[n * cap : (n + 1) * cap]
-    for d in range(1, nsp):
-        n = (s + d) % nsp
-        send(outgo.at[n], xbuf.at[y, s], d_s.at[d], d_r.at[s], sp_dev(n))
+    near = s // cb
+
+    def dispatch(n):
+        send(outgo.at[n], xbuf.at[y, s], d_s.at[n], d_r.at[s], sp_dev(n))
+
+    for d in range(1, cb):
+        dispatch(near * cb + (s + d) % cb)
+    for i in range(cb):
+        for d in (NCH - 1, 1)[: NCH - 1]:
+            dispatch((near + d) % NCH * cb + i)
+    for d in range(2, NCH - 1):
+        for i in range(cb):
+            dispatch((near + d) % NCH * cb + i)
     xbuf[y, s] = outgo[s]
+    later_weights()
 
     for d in range(1, nx):
         n = (x + d) % nx
@@ -461,8 +529,6 @@
     for d in range(1, ny):
         n = (y + d) % ny
         landed(wd.at[n], wd_r.at[n])
-
-    near = s // cb
 
     def chunk(k):
         return (near + k + k // 2 - 2 * (k // 3)) % NCH
@@ -551,6 +617,7 @@
             def _():
                 ret[s] = eout[b]
 
+
     stages = (stage_a, stage_b, stage_c, stage_d, stage_e)
 
     def step(i, carry):
@@ -568,26 +635,31 @@
         n = (s + d) % nsp
         landed(ret.at[n], b_r.at[n])
     back = ret[...].reshape(nsp * cap, FW)
-    gap = rl_ref[:, 0:1] - rl_ref[:, 1:2]
+    gap = rl_ref[0:1] - rl_ref[1:2]
     w0 = gw_ref[...] / (1.0 + jnp.exp(-gap))
     w1 = gw_ref[...] / (1.0 + jnp.exp(gap))
-    routed = w0 * dot_n(sel0[...], back) + w1 * dot_n(sel1[...], back)
+    both = jnp.where(row_t == 0, w0, jnp.where(row_t == 1, w1, 0.0))
+    w0, w1 = dot_exact(both, pick_a, first), dot_exact(both, pick_b, first)
+    w0, w1 = jnp.concatenate([w0, w0], axis=1), jnp.concatenate([w1, w1], axis=1)
+    routed = w0 * flipped(sel0[...], back) + w1 * flipped(sel1[...], back)
     o_ref[...] = (stream[...] + routed).astype(bf16)
 
     for copy in sends:
         copy.wait_send()
 
-    @pl.when(source)
-    def _():
-        for n in range(nz):
-            landed(kv_ref, kv_s.at[n])
-
-    for i in range(nb):
-        relay = (c == i % 2) & (z != (i * grp + j) // 2)
-
-        @pl.when(relay)
+    for part, (src, dst) in enumerate(kv_pairs):
+
+        @pl.when(source)
         def _():
-            landed(kvbuf.at[i], kv_f.at[i])
+            for n in range(nz):
+                landed(src, kv_s.at[part, n])
+
+        for i in range(nb):
+            relay = (c == i % 2) & (z != (i * grp + j) // 2)
+
+            @pl.when(relay)
+            def _():
+                landed(dst.at[i], kv_f.at[part, i])
 
     for d in range(1, grp):
         g = (j + d) % grp
@@ -634,49 +706,21 @@
     cb = nsp // NCH
     rows = cb * cap
     bf16, f32 = jnp.bfloat16, jnp.float32
-    s = lax.axis_index("z") * 2 + lax.axis_index("c")
-    head = lax.axis_index("y") // half
-    positions = s * t + jnp.arange(t, dtype=jnp.int32)
-
-    def own(array):
-        return lax.dynamic_index_in_dim(array, head, 1, keepdims=False)
-
-    q_all = jnp.concatenate(
-        [
-            prepare(lean_query[:, 0], lean_gains[0], positions),
-            jnp.zeros((t, HA), bf16),
-            prepare(broad_query[:, 0], broad_gains[0], positions),
-        ],
-        axis=1,
-    )
-    kv_all = jnp.concatenate(
-        [
-            prepare(own(lean_key), lean_gains[1], positions),
-            own(lean_value),
-            prepare(own(broad_key), broad_gains[1], positions),
-            own(broad_value),
-        ],
-        axis=1,
-    )
-    gains = jnp.concatenate(
-        [
-            jnp.zeros((ntp, HA), f32),
-            mixer_gain[: ntp * HA].reshape(ntp, HA),
-            mixer_gain[ntp * HA :].reshape(ntp, HB),
-        ],
-        axis=1,
-    ).reshape(ntp, 1, FW)
     vm = pl.BlockSpec(memory_space=pltpu.VMEM)
     hbm = pl.BlockSpec(memory_space=pl.ANY)
     dma = pltpu.SemaphoreType.DMA
     return pl.pallas_call(
         functools.partial(layer_kernel, (nz, ny, nx, t, cap)),
         out_shape=jax.ShapeDtypeStruct((t, FW), bf16),
-        in_specs=[vm, vm, vm, hbm, hbm, hbm, hbm, hbm, vm, vm, vm, vm, vm],
+        in_specs=[vm] * 9 + [hbm] * 5 + [vm] * 5,
         out_specs=vm,
         scratch_shapes=[
+            pltpu.VMEM((t, 256), bf16),
+            pltpu.VMEM((t, 128), bf16),
+            pltpu.VMEM((t, 256), bf16),
             pltpu.VMEM((grp, t, 256), bf16),
-            pltpu.VMEM((nb, t, 384), bf16),
+            pltpu.VMEM((nb, t, 128), bf16),
+            pltpu.VMEM((nb, t, 256), bf16),
             pltpu.VMEM((grp, t, 256), bf16),
             pltpu.VMEM((grp, t, 256), bf16),
             pltpu.VMEM((ny, nx, 4, 64, FW), bf16),
@@ -691,8 +735,8 @@
             pltpu.VMEM((8, 256), f32),
             pltpu.VMEM((ntp, 8, 256), f32),
             pltpu.VMEM((t, FW), f32),
-            pltpu.VMEM((t, nsp * cap), bf16),
-            pltpu.VMEM((t, nsp * cap), bf16),
+            pltpu.VMEM((nsp * cap, t), bf16),
+            pltpu.VMEM((nsp * cap, t), bf16),
             pltpu.VMEM((nsp, cap, FW), bf16),
             pltpu.VMEM((ny, nsp, cap, FW), bf16),
             pltpu.VMEM((NCH, nx, rows, FW), bf16),
@@ -706,9 +750,9 @@
             pltpu.VMEM((nsp, cap, FW), bf16),
             dma((grp,)),
             dma((grp,)),
-            dma((nz,)),
-            dma((nb,)),
-            dma((nb,)),
+            dma((2, nz)),
+            dma((2, nb)),
+            dma((2, nb)),
             dma((grp,)),
             dma((grp,)),
             dma((2, ny)),
@@ -743,19 +787,25 @@
             collective_id=0, has_side_effects=True, vmem_limit_bytes=60 * 1024 * 1024
         ),
     )(
-        q_all,
-        kv_all,
+        lean_query.transpose(1, 2, 0)[0],
+        lean_key.transpose(1, 2, 0),
+        lean_value.transpose(1, 2, 0),
+        lean_gains,
+        broad_query[:, 0],
+        broad_key.reshape(KV * t, HB),
+        broad_value.reshape(KV * t, HB),
+        broad_gains,
         tokens,
         output_weight.reshape(3 * ntp, 64, FW),
         output_weight.reshape(3 * ntp // 2, 2, 64, FW),
         gate_weight.reshape(ny, nx, FW, FE),
         up_weight.reshape(ny, nx, FW, FE),
         down_weight.reshape(ny, nx * FE, FW),
-        gains,
+        mixer_gain.reshape(-1, 128),
         channel_gain.reshape(1, FW),
-        route_experts,
-        route_logits,
-        group_weight.reshape(t, 1),
+        route_experts.T,
+        route_logits.T,
+        group_weight.reshape(1, t),
     )
 
 

time: 177 us -> 151 us (0.85)
  Pallas kernels: 161 us -> 148 us
  local copies, waits for them, and re-layouts: 8.56 us -> 1.54 us
  other arithmetic: 4.26 us -> 0 us
    pallas_call x1, Pallas kernels: 161 us -> 148 us  [on_device(): pl.pallas_call(functools.partial(layer_kernel, (nz, ny, nx, t, cap)), out...]
    unnamed x22 -> x1, local copies, waits for them, and re-layouts: 3.34 us -> 1.54 us
where the time goes in v2:
time: 151 us; the launch traced here: 149 us
  Pallas kernels  148 us (98%)
  local copies, waits for them, and re-layouts  1.54 us (1%)
    pallas_call x1, Pallas kernels, on_device(): pl.pallas_call(functools.partial(layer_kernel, (nz, ny, nx, t, cap)), out...  148 us

profile of v2, /device:TPU:1, one launch (start us, length us, event | category | flops | bytes accessed | tf_op | source)
XLA Modules:
  0.0 149.2 jit_solution(258203745056504722)
XLA Ops:
  0.0 147.6 %shard_map.172 = bf16[192,256]{1,0:T(8,128)(2,1)} custom-call(bf16[64,192]{1,0:T(8,128)(2,1)} %bitcast.28, bf16[2,64,192]{2,1,0:T(8,128)(2,1)} %bitcast.25, bf16[2,64,192]{2,1,0:T(8,128)(2,1)} %bitcast.26, f32[2,64]{1,0:T(2,128)} %lg_ref.1, bf16[192,128]{1,0:T(8,128)(2,1)} %bitcast.27, bf16[384,128]{1,0:T(8,128)(2,1)} %bitcast.23, ...), custom_call_target="tpu_custom_call" | custom-call | tf_op jit(solution)/shard_map/pallas_call | solution.py:712
  147.6 1.5 %copy.20 = bf16[192,256]{1,0:T(8,128)(2,1)} copy(bf16[192,256]{1,0:T(8,128)(2,1)} %shard_map.172) | data formatting | bytes 196608

commit v3 on v2

--- a/solution.py
+++ b/solution.py
@@ -16,6 +16,8 @@
 GROUPS = 4
 NY, NX = 4, 4
 NCH = 4
+HUBS = (8, 5, 11, 2, 14)
+UNROLL = 2
 HA, HB = 64, 128
 FW = 256
 FE = 128
@@ -86,8 +88,12 @@
     qbuf,
     kvl,
     kvb,
-    osend,
-    obuf,
+    osl,
+    osb,
+    obl,
+    obb,
+    lsend,
+    lbuf,
     wo,
     wgu,
     wd,
@@ -102,6 +108,9 @@
     stream,
     sel0,
     sel1,
+    sel_wide,
+    scsend,
+    scbuf,
     outgo,
     xbuf,
     rsend,
@@ -137,6 +146,8 @@
     st2_r,
     d_s,
     d_r,
+    sc_s,
+    sc_r,
     ya_s,
     ya_r,
     rx_s,
@@ -152,20 +163,22 @@
     nsp = nz * 2
     ntp = ny * nx
     half = ny // KV
-    grp = half * nx
+    grp = nx
     nb = nsp // grp
     cb = nsp // NCH
     rows = cb * cap
+    wide = 32 if cap <= 32 else 128
+    per = 128 // wide
     z, c = lax.axis_index("z"), lax.axis_index("c")
     y, x = lax.axis_index("y"), lax.axis_index("x")
     s = z * 2 + c
     tp = y * nx + x
     head = y // half
-    j = (y % half) * nx + x
+    j = x
     bf16, f32 = jnp.bfloat16, jnp.float32
 
     def member(g):
-        return (z, c, head * half + g // nx, g % nx)
+        return (z, c, y, g)
 
     def tp_dev(n):
         return (z, c, n // nx, n % nx)
@@ -243,12 +256,18 @@
     before = (
         lax.broadcasted_iota(jnp.int32, (t, t), 0) < lax.broadcasted_iota(jnp.int32, (t, t), 1)
     ).astype(bf16)
-    rank = dot_n((e0 + e1).astype(bf16), before) + (experts * cap).astype(f32)
-    slot_row = lax.broadcasted_iota(jnp.int32, (nsp * cap, t), 0)
-    slot0 = jnp.sum(e0 * rank, axis=0, keepdims=True).astype(jnp.int32)
-    slot1 = jnp.sum(e1 * rank, axis=0, keepdims=True).astype(jnp.int32)
-    sel0[...] = (slot_row == slot0).astype(f32).astype(bf16)
-    sel1[...] = (slot_row == slot1).astype(f32).astype(bf16)
+    rank = dot_n((e0 + e1).astype(bf16), before)
+
+    def slots(pitch):
+        row = lax.broadcasted_iota(jnp.int32, (nsp * pitch, t), 0)
+        place = rank + (experts * pitch).astype(f32)
+        for e in (e0, e1):
+            slot = jnp.sum(e * place, axis=0, keepdims=True).astype(jnp.int32)
+            yield (row == slot).astype(f32)
+
+    for part, sel in zip(slots(cap), (sel0, sel1)):
+        sel[...] = part.astype(bf16)
+    sel_wide[...] = sum(slots(wide)).astype(bf16)
     wo[:, :, 0] = jnp.zeros_like(wo[:, :, 0])
     qbuf[j] = q_ref[...]
 
@@ -263,15 +282,13 @@
 
     source = s % grp == j
     mine = s // grp
-    order = [nz // 2]
-    for d in range(nz // 2 - 1, 0, -1):
-        order += [d, nz - d]
+    hubs = HUBS if nz == 16 else tuple(range(1, nz))
     kv_pairs = ((kvl_ref, kvl), (kvb_ref, kvb))
 
     @pl.when(source)
     def _():
         for part, (src, dst) in enumerate(kv_pairs):
-            for n, d in enumerate(order):
+            for n, d in enumerate(hubs):
                 rcopy(
                     src,
                     dst.at[mine],
@@ -313,41 +330,69 @@
         dev = (z, c, y, to)
         send(gate_ref.at[:, to], wgu.at[x, :, :, pl.ds(0, FE)], wg_s.at[0, d], wg_r.at[0, x], dev)
 
-    def later_weights():
-        for d in range(1, nx):
-            to = (x + d) % nx
-            dev = (z, c, y, to)
-            send(
-                up_ref.at[:, to], wgu.at[x, :, :, pl.ds(FE, FE)], wg_s.at[1, d], wg_r.at[1, x], dev
-            )
-        for d in range(1, ny):
-            to = (y + d) % ny
-            send(down_ref.at[to], wd.at[y], wd_s.at[d], wd_r.at[y], (z, c, to, x))
+    def send_up(d):
+        to = (x + d) % nx
+        dev = (z, c, y, to)
+        send(up_ref.at[:, to], wgu.at[x, :, :, pl.ds(FE, FE)], wg_s.at[1, d], wg_r.at[1, x], dev)
+
+    near_x = sorted({1, nx - 1})
+    for d in near_x:
+        send_up(d)
+
+    for d in range(1, ny):
+        to = (y + d) % ny
+        send(down_ref.at[to], wd.at[y], wd_s.at[d], wd_r.at[y], (z, c, to, x))
 
     local(up_ref.at[:, x], wgu.at[x, :, :, pl.ds(FE, FE)], 3)
     local(down_ref.at[y], wd.at[y], 4)
 
-    def arrive(part):
+    def away(i):
+        return (z - (i * grp + j) // 2 + nz) % nz
+
+    def hub(i):
+        return (c == i % 2) & (away(i) % 3 == 2) if nz == 16 else away(i) < 0
+
+    def pass_on(part, i):
+        dst = kv_pairs[part][1]
+        landed(dst.at[i], kv_r.at[part, i])
+
+        @pl.when((c == i % 2) & (away(i) != 0))
+        def _():
+            rcopy(
+                dst.at[i], dst.at[i], kv_f.at[part, i, 0], kv_r.at[part, i], (z, 1 - c, y, x)
+            ).start()
+
+    def arrive_first(part):
         src, dst = kv_pairs[part]
         for i in range(nb):
-            own = (mine == i) & source
-            relay = (c == i % 2) & (z != (i * grp + j) // 2)
-
-            @pl.when(own)
+
+            @pl.when((mine == i) & source)
             def _():
                 dst[i] = src[...]
 
-            @pl.when(jnp.logical_not(own))
-            def _():
-                landed(dst.at[i], kv_r.at[part, i])
-
-            @pl.when(relay)
-            def _():
-                rcopy(
-                    dst.at[i], dst.at[i], kv_f.at[part, i], kv_r.at[part, i], (z, 1 - c, y, x)
-                ).start()
-
+            @pl.when(hub(i))
+            def _():
+                pass_on(part, i)
+                for n, d in ((1, 1), (2, nz - 1)):
+                    rcopy(
+                        dst.at[i],
+                        dst.at[i],
+                        kv_f.at[part, i, n],
+                        kv_r.at[part, i],
+                        ((z + d) % nz, c, y, x),
+                    ).start()
+
+    def arrive(part):
+        for i in range(nb):
+            direct = ((mine == i) & source) | hub(i)
+
+            @pl.when(jnp.logical_not(direct))
+            def _():
+                pass_on(part, i)
+
+    arrive_first(0)
     arrive(0)
+    arrive_first(1)
     for d in range(1, grp):
         g = (j + d) % grp
         landed(qbuf.at[g], q_r.at[g])
@@ -373,46 +418,63 @@
             value = jnp.where(lane_a == at + n, piece, value)
         return value
 
-    def lean_head(g, carry):
+    def hand_over(part, src, dst, d, g):
+        @pl.when(d < grp)
+        def _():
+            rcopy(src.at[g], dst.at[j], o_s.at[part, g], o_r.at[part, j], member(g)).start()
+
+        @pl.when(d == grp)
+        def _():
+            dst[j] = src[g]
+
+    def lean_head(d, carry):
+        g = (j + d) % grp
         kv_l = kvl[...].reshape(nb * t, 128)
         out, lse = attend(dot_t(qbuf[g, :, 0:128], kv_l), kv_l, scale_a)
-        osend[g, :, 0:128] = marked(out, lse, 0).astype(bf16)
+        osl[g] = marked(out, lse, 0).astype(bf16)
+        hand_over(0, osl, obl, d, g)
         return carry
 
-    def broad_head(d, carry):
+    def broad_head(d, lses):
         g = (j + d) % grp
         k_b = kvb[:, :, 0:128].reshape(nb * t, 128)
         v_b = kvb[:, :, 128:256].reshape(nb * t, 128)
         out, lse = attend(dot_t(qbuf[g, :, 128:256], k_b), v_b, scale_b)
-        osend[g, :, 0:128] = marked(osend[g, :, 0:128].astype(f32), lse, 3).astype(bf16)
-        osend[g, :, 128:256] = out.astype(bf16)
-
-        @pl.when(d < grp)
-        def _():
-            rcopy(osend.at[g], obuf.at[j], o_s.at[g], o_r.at[j], member(g)).start()
-
-        @pl.when(d == grp)
-        def _():
-            obuf[j] = osend[g]
-
-        return carry
-
-    lax.fori_loop(0, grp, lean_head, 0)
+        osb[g] = out.astype(bf16)
+        hand_over(1, osb, obb, d, g)
+        return jnp.where(lane_a == g, lse, lses)
+
+    lax.fori_loop(1, grp + 1, lean_head, 0, unroll=UNROLL)
     arrive(1)
-    lax.fori_loop(1, grp + 1, broad_head, 0)
-
+    lses = lax.fori_loop(1, grp + 1, broad_head, jnp.zeros((t, 128), f32), unroll=UNROLL)
+    last = ((1,), (1,))
+    row8 = lax.broadcasted_iota(jnp.int32, (8, 128), 0)
+    eye8 = (row8 == lax.broadcasted_iota(jnp.int32, (8, 128), 1)).astype(f32)
+    lsend[...] = jnp.zeros_like(lsend)
+    lse_rows = dot_exact(eye8, lses, last)
+    for g in range(grp):
+        lsend[g, :, 0:t] = lse_rows[g : g + 1]
     for d in range(1, grp):
         g = (j + d) % grp
-        landed(obuf.at[g], o_r.at[g])
-
+        send(lsend.at[g], lbuf.at[j], o_s.at[2, g], o_r.at[2, j], member(g))
+    lbuf[j] = lsend[j]
+
+    for d in range(1, grp):
+        g = (j + d) % grp
+        landed(obl.at[g], o_r.at[0, g])
+        landed(obb.at[g], o_r.at[1, g])
+        landed(lbuf.at[g], o_r.at[2, g])
+
+    row_g = lax.broadcasted_iota(jnp.int32, (8, t), 0)
+    lse_rows = jnp.zeros((8, t), f32)
+    for g in range(grp):
+        lse_rows = jnp.where(row_g == g, lbuf[g, :, 0:t], lse_rows)
+    lse_cols = dot_exact(lse_rows, eye8, first)
     lses = []
     for g in range(grp):
-        stats = obuf[g, :, 0:128].astype(f32)
+        stats = obl[g].astype(f32)
         lses.append(
-            (
-                stats[:, 0:1] + stats[:, 1:2] + stats[:, 2:3],
-                stats[:, 3:4] + stats[:, 4:5] + stats[:, 5:6],
-            )
+            (stats[:, 0:1] + stats[:, 1:2] + stats[:, 2:3], lse_cols[:, g : g + 1])
         )
     top_a = functools.reduce(jnp.maximum, [v[0] for v in lses])
     top_b = functools.reduce(jnp.maximum, [v[1] for v in lses])
@@ -422,19 +484,18 @@
         wa = jnp.exp2(lses[g][0] - top_a)
         wb = jnp.exp2(lses[g][1] - top_b)
         sum_a, sum_b = sum_a + wa, sum_b + wb
-        acc_a = acc_a + wa * obuf[g, :, 0:128].astype(f32)
-        acc_b = acc_b + wb * obuf[g, :, 128:256].astype(f32)
+        acc_a = acc_a + wa * obl[g].astype(f32)
+        acc_b = acc_b + wb * obb[g].astype(f32)
     head_a = jnp.where(lane_a >= HA, acc_a / sum_a, 0.0).astype(bf16)
     head_b = (acc_b / sum_b).astype(bf16)
     msend[:, 0:128] = head_a
     msend[:, 128:256] = head_b
-    row8 = lax.broadcasted_iota(jnp.int32, (8, 128), 0)
     pick_a = (row8 == 0).astype(f32)
     pick_b = (row8 == 1).astype(f32)
     sq_a, sq_b = head_a.astype(f32), head_b.astype(f32)
-    last = ((1,), (1,))
     stsend[...] = jnp.zeros_like(stsend)
-    stsend[:, 0:t] = dot_exact(pick_a, sq_a * sq_a, last) + dot_exact(pick_b, sq_b * sq_b, last)
+    squares = dot_exact(pick_a, sq_a * sq_a, last) + dot_exact(pick_b, sq_b * sq_b, last)
+    stsend[:, 0:t] = squares[0:2]
     for d in range(1, ntp):
         n = (tp + d) % ntp
         send(stsend, stbuf.at[tp], st_s.at[d], st_r.at[tp], tp_dev(n))
@@ -448,8 +509,8 @@
         landed(stbuf.at[n], st_r.at[n])
     sums = jnp.sum(stbuf[...], axis=0)[:, 0:t]
     row_t = lax.broadcasted_iota(jnp.int32, (8, t), 0)
-    width = jnp.where(row_t == 0, 1.0 / (ntp * HA), 1.0 / (ntp * HB))
-    inverse = lax.rsqrt(sums * width + epsilon)
+    sums = jnp.where(row_t == 0, sums[0:1] * (1.0 / (ntp * HA)), sums[1:2] * (1.0 / (ntp * HB)))
+    inverse = lax.rsqrt(sums + epsilon)
     norm_a = dot_exact(inverse, pick_a, first)
     norm_b = dot_exact(inverse, pick_b, first)
     for d in range(1, nx):
@@ -480,6 +541,9 @@
         to = (y + d) % ny
         psend[d] = project(to).astype(bf16)
         send(psend.at[d], pbuf.at[y], p_s.at[d], p_r.at[y], (z, c, to, x))
+    for d in range(1, nx):
+        if d not in near_x:
+            send_up(d)
     total = tok_ref[...].astype(f32) + project(y)
     for d in range(1, ny):
         n = (y + d) % ny
@@ -488,50 +552,53 @@
     stream[...] = total
     ones8 = jnp.ones((8, FW), f32)
     st2send[...] = jnp.zeros_like(st2send)
-    st2send[:, 0:t] = dot_exact(ones8, total * total, last)
+    st2send[:, 0:t] = dot_exact(ones8, total * total, last)[0:1]
     for d in range(1, ntp):
         n = (tp + d) % ntp
         send(st2send, st2buf.at[tp], st2_s.at[d], st2_r.at[tp], tp_dev(n))
     st2buf[tp] = st2send[...]
+
+    feats = (total * cg_ref[...]).astype(bf16)
+    picked = dot_n(sel0[...] + sel1[...], feats).astype(bf16)
+    for n in range(nsp):
+        outgo[n] = picked[n * cap : (n + 1) * cap]
+    near = s // cb
+
+    def dispatch(n):
+        copy = rcopy(outgo.at[n], xbuf.at[y, s], d_s.at[n], d_r.at[s], sp_dev(n))
+        copy.start()
+        return copy
+
+    def dispatch_far(far):
+        for i in range(cb):
+            for d in sorted({NCH - far, far}, reverse=True):
+                sends.append(dispatch((near + d) % NCH * cb + i))
+
+    for copy in [dispatch(near * cb + (s + d) % cb) for d in range(1, cb)]:
+        copy.wait_send()
+    xbuf[y, s] = outgo[s]
+    for far in range(1, NCH // 2):
+        dispatch_far(far)
     for d in range(1, ntp):
         n = (tp + d) % ntp
         landed(st2buf.at[n], st2_r.at[n])
     squares = jnp.sum(st2buf[...], axis=0)[:, 0:t]
     inverse = lax.rsqrt(squares * (1.0 / (ntp * FW)) + epsilon)
-    norm = dot_exact(inverse, jnp.where(row8 == 0, 1.0, 0.0), first)
-    normed = (
-        stream[...] * jnp.concatenate([norm, norm], axis=1) * cg_ref[...]
-    ).astype(bf16)
-
-    picked = dot_n(sel0[...] + sel1[...], normed).astype(bf16)
-    for n in range(nsp):
-        outgo[n] = picked[n * cap : (n + 1) * cap]
-    near = s // cb
-
-    def dispatch(n):
-        send(outgo.at[n], xbuf.at[y, s], d_s.at[n], d_r.at[s], sp_dev(n))
-
-    for d in range(1, cb):
-        dispatch(near * cb + (s + d) % cb)
-    for i in range(cb):
-        for d in (NCH - 1, 1)[: NCH - 1]:
-            dispatch((near + d) % NCH * cb + i)
-    for d in range(2, NCH - 1):
-        for i in range(cb):
-            dispatch((near + d) % NCH * cb + i)
-    xbuf[y, s] = outgo[s]
-    later_weights()
-
-    for d in range(1, nx):
-        n = (x + d) % nx
-        landed(wgu.at[n, :, :, pl.ds(0, FE)], wg_r.at[0, n])
-        landed(wgu.at[n, :, :, pl.ds(FE, FE)], wg_r.at[1, n])
-    for d in range(1, ny):
-        n = (y + d) % ny
-        landed(wd.at[n], wd_r.at[n])
+    inverse = jnp.broadcast_to(inverse, (8, t))
+    parts = split3(inverse)
+    split = jnp.where(row_t == 0, parts[0], jnp.where(row_t == 1, parts[1], parts[2]))
+    split = jnp.where(row_t < 3, split, 0.0).astype(bf16)
+    factors = jnp.sum(dot_t(split, sel_wide[...]), axis=0, keepdims=True)
+    for n in range(nsp // per):
+        scsend[n] = factors[:, n * 128 : (n + 1) * 128]
+    for d in range(1, nsp):
+        n = (s + d) % nsp
+        send(scsend.at[n // per], scbuf.at[s], sc_s.at[d], sc_r.at[s], sp_dev(n))
+    scbuf[s] = scsend[s // per]
+    dispatch_far(NCH // 2)
 
     def chunk(k):
-        return (near + k + k // 2 - 2 * (k // 3)) % NCH
+        return (near + NCH + (k + 1) // 2 * (2 * (k % 2) - 1)) % NCH
 
     def stage_a(k):
         ch = chunk(k)
@@ -552,6 +619,14 @@
         for d in range(1, ny):
             n = (y + d) % ny
             landed(xbuf.at[n, pl.ds(ch * cb, cb)], ya_r.at[ch, n])
+
+        @pl.when(k == 0)
+        def _():
+            for d in range(1, nx):
+                n = (x + d) % nx
+                landed(wgu.at[n, :, :, pl.ds(0, FE)], wg_r.at[0, n])
+                landed(wgu.at[n, :, :, pl.ds(FE, FE)], wg_r.at[1, n])
+
         xs = [xbuf[n, pl.ds(ch * cb, cb)].reshape(rows, FW) for n in range(ny)]
 
         def expand(n):
@@ -575,6 +650,19 @@
             n = (x + d) % nx
             landed(rbuf.at[ch, n], rx_r.at[ch, n])
             both = both + rbuf[ch, n].astype(f32)
+        row = lax.broadcasted_iota(jnp.int32, (cap, 128), 0)
+        spot = row + s % per * wide == lax.broadcasted_iota(jnp.int32, (cap, 128), 1)
+        factor = []
+        for i in range(cb):
+            b = ch * cb + i
+
+            @pl.when(b != s)
+            def _():
+                landed(scbuf.at[b], sc_r.at[b])
+
+            value = jnp.where(spot, scbuf[b], 0.0)
+            factor.append(jnp.sum(value, axis=1, keepdims=True))
+        both = both * jnp.concatenate(factor, axis=0)
         gate_value = both[:, 0:FE]
         hidden = (gate_value / (1.0 + jnp.exp(-gate_value)) * both[:, FE:]).astype(bf16)
         hbuf[ch, x] = hidden
@@ -589,6 +677,13 @@
         for d in range(1, nx):
             n = (x + d) % nx
             landed(hbuf.at[ch, n], hx_r.at[ch, n])
+
+        @pl.when(k == 0)
+        def _():
+            for d in range(1, ny):
+                n = (y + d) % ny
+                landed(wd.at[n], wd_r.at[n])
+
         wide = jnp.concatenate([hbuf[ch, n] for n in range(nx)], axis=1)
         for d in range(1, ny):
             to = (y + d) % ny
@@ -620,12 +715,27 @@
 
     stages = (stage_a, stage_b, stage_c, stage_d, stage_e)
 
+    ahead = ((1, 1), (1, 2)) if NCH == 4 else ()
+    behind = ((0, 0), (2, 3)) if NCH == 4 else tuple((k, k) for k in range(NCH))
+
     def step(i, carry):
-        for lag, stage in enumerate(stages):
+        for at, k in ahead:
+
+            @pl.when(i == at)
+            def _():
+                stage_a(k)
+
+        for lag in (4, 3, 2, 1):
 
             @pl.when((i >= lag) & (i < NCH + lag))
             def _():
-                stage(i - lag)
+                stages[lag](i - lag)
+
+        for at, k in behind:
+
+            @pl.when(i == at)
+            def _():
+                stage_a(k)
 
         return carry
 
@@ -651,7 +761,7 @@
 
         @pl.when(source)
         def _():
-            for n in range(nz):
+            for n in (*range(len(hubs)), nz - 1):
                 landed(src, kv_s.at[part, n])
 
         for i in range(nb):
@@ -659,11 +769,17 @@
 
             @pl.when(relay)
             def _():
-                landed(dst.at[i], kv_f.at[part, i])
+                landed(dst.at[i], kv_f.at[part, i, 0])
+
+            @pl.when(hub(i))
+            def _():
+                for n in (1, 2):
+                    landed(dst.at[i], kv_f.at[part, i, n])
 
     for d in range(1, grp):
         g = (j + d) % grp
-        landed(osend.at[g], o_s.at[g])
+        landed(osl.at[g], o_s.at[0, g])
+        landed(osb.at[g], o_s.at[1, g])
     for ch in range(NCH):
         for d in range(1, ny):
             landed(xbuf.at[y, pl.ds(ch * cb, cb)], ya_s.at[ch, d])
@@ -700,8 +816,9 @@
     nsp, ntp = nz * 2, ny * nx
     t = tokens.shape[0]
     cap = t // (nsp // GROUPS)
+    wide = 32 if cap <= 32 else 128
     half = ny // KV
-    grp = half * nx
+    grp = nx
     nb = nsp // grp
     cb = nsp // NCH
     rows = cb * cap
@@ -721,22 +838,29 @@
             pltpu.VMEM((grp, t, 256), bf16),
             pltpu.VMEM((nb, t, 128), bf16),
             pltpu.VMEM((nb, t, 256), bf16),
-            pltpu.VMEM((grp, t, 256), bf16),
-            pltpu.VMEM((grp, t, 256), bf16),
+            pltpu.VMEM((grp, t, 128), bf16),
+            pltpu.VMEM((grp, t, 128), bf16),
+            pltpu.VMEM((grp, t, 128), bf16),
+            pltpu.VMEM((grp, t, 128), bf16),
+            pltpu.VMEM((8, 1, 256), f32),
+            pltpu.VMEM((grp, 1, 256), f32),
             pltpu.VMEM((ny, nx, 4, 64, FW), bf16),
             pltpu.VMEM((nx, ny, FW, FW), bf16),
             pltpu.VMEM((ny, nx * FE, FW), bf16),
             pltpu.VMEM((t, 256), bf16),
             pltpu.VMEM((nx, t, 256), bf16),
-            pltpu.VMEM((8, 256), f32),
-            pltpu.VMEM((ntp, 8, 256), f32),
+            pltpu.VMEM((2, 256), f32),
+            pltpu.VMEM((ntp, 2, 256), f32),
             pltpu.VMEM((ny, t, FW), bf16),
             pltpu.VMEM((ny, t, FW), bf16),
-            pltpu.VMEM((8, 256), f32),
-            pltpu.VMEM((ntp, 8, 256), f32),
+            pltpu.VMEM((1, 256), f32),
+            pltpu.VMEM((ntp, 1, 256), f32),
             pltpu.VMEM((t, FW), f32),
             pltpu.VMEM((nsp * cap, t), bf16),
             pltpu.VMEM((nsp * cap, t), bf16),
+            pltpu.VMEM((nsp * wide, t), bf16),
+            pltpu.VMEM((nsp * wide // 128, 1, 128), f32),
+            pltpu.VMEM((nsp, 1, 128), f32),
             pltpu.VMEM((nsp, cap, FW), bf16),
             pltpu.VMEM((ny, nsp, cap, FW), bf16),
             pltpu.VMEM((NCH, nx, rows, FW), bf16),
@@ -752,9 +876,9 @@
             dma((grp,)),
             dma((2, nz)),
             dma((2, nb)),
-            dma((2, nb)),
-            dma((grp,)),
-            dma((grp,)),
+            dma((2, nb, 3)),
+            dma((3, grp)),
+            dma((3, grp)),
             dma((2, ny)),
             dma((2, ny)),
             dma((2, nx)),
@@ -770,6 +894,8 @@
             dma((ny,)),
             dma((ntp,)),
             dma((ntp,)),
+            dma((nsp,)),
+            dma((nsp,)),
             dma((nsp,)),
             dma((nsp,)),
             dma((NCH, ny)),

time: 151 us -> 146 us (0.967)
  Pallas kernels: 148 us -> 144 us
    pallas_call x1, Pallas kernels: 148 us -> 144 us  [on_device(): pl.pallas_call(functools.partial(layer_kernel, (nz, ny, nx, t, cap)), out...]
where the time goes in v3:
time: 146 us; the launch traced here: 145 us
  Pallas kernels  144 us (99%)
  local copies, waits for them, and re-layouts  1.54 us (1%)
    pallas_call x1, Pallas kernels, on_device(): pl.pallas_call(functools.partial(layer_kernel, (nz, ny, nx, t, cap)), out...  144 us

profile of v3, /device:TPU:1, one launch (start us, length us, event | category | flops | bytes accessed | tf_op | source)
XLA Modules:
  0.0 145.1 jit_solution(2001803063446383552)
XLA Ops:
  0.0 143.5 %shard_map.172 = bf16[192,256]{1,0:T(8,128)(2,1)} custom-call(bf16[64,192]{1,0:T(8,128)(2,1)} %bitcast.28, bf16[2,64,192]{2,1,0:T(8,128)(2,1)} %bitcast.25, bf16[2,64,192]{2,1,0:T(8,128)(2,1)} %bitcast.26, f32[2,64]{1,0:T(2,128)} %lg_ref.1, bf16[192,128]{1,0:T(8,128)(2,1)} %bitcast.27, bf16[384,128]{1,0:T(8,128)(2,1)} %bitcast.23, ...), custom_call_target="tpu_custom_call" | custom-call | tf_op jit(solution)/shard_map/pallas_call | solution.py:829
  143.5 1.5 %copy.20 = bf16[192,256]{1,0:T(8,128)(2,1)} copy(bf16[192,256]{1,0:T(8,128)(2,1)} %shard_map.172) | data formatting | bytes 196608

commit v4 on v3

--- a/solution.py
+++ b/solution.py
@@ -273,12 +273,9 @@
 
     pl.semaphore_wait(barrier, nsp - 1 + ntp - 1)
 
-    sends = []
-
     def send(src, dst, send_sem, recv_sem, device):
         copy = rcopy(src, dst, send_sem, recv_sem, device)
         copy.start()
-        sends.append(copy)
 
     source = s % grp == j
     mine = s // grp
@@ -292,17 +289,17 @@
                 rcopy(
                     src,
                     dst.at[mine],
-                    kv_s.at[part, n],
+                    kv_s.at[part],
                     kv_r.at[part, mine],
                     ((z + d) % nz, mine % 2, y, x),
                 ).start()
             rcopy(
-                src, dst.at[mine], kv_s.at[part, nz - 1], kv_r.at[part, mine], (z, 1 - c, y, x)
+                src, dst.at[mine], kv_s.at[part], kv_r.at[part, mine], (z, 1 - c, y, x)
             ).start()
 
     for d in range(1, grp):
         g = (j + d) % grp
-        send(q_ref, qbuf.at[j], q_s.at[d], q_r.at[j], member(g))
+        send(q_ref, qbuf.at[j], q_s.at[0], q_r.at[0], member(g))
 
     locals_ = []
 
@@ -317,23 +314,23 @@
     for d in range(1, ny):
         to = (y + d) % ny
         dev = (z, c, to, x)
-        send(wl_ref.at[pl.ds(to * nx, nx)], wo.at[y, :, 1], wo_s.at[0, d], wo_r.at[0, y], dev)
+        send(wl_ref.at[pl.ds(to * nx, nx)], wo.at[y, :, 1], wo_s.at[0], wo_r.at[0], dev)
         send(
             wb_ref.at[pl.ds(ntp // 2 + to * nx, nx)],
             wo.at[y, :, pl.ds(2, 2)],
-            wo_s.at[1, d],
-            wo_r.at[1, y],
+            wo_s.at[1],
+            wo_r.at[1],
             dev,
         )
     for d in range(1, nx):
         to = (x + d) % nx
         dev = (z, c, y, to)
-        send(gate_ref.at[:, to], wgu.at[x, :, :, pl.ds(0, FE)], wg_s.at[0, d], wg_r.at[0, x], dev)
+        send(gate_ref.at[:, to], wgu.at[x, :, :, pl.ds(0, FE)], wg_s.at[0], wg_r.at[0], dev)
 
     def send_up(d):
         to = (x + d) % nx
         dev = (z, c, y, to)
-        send(up_ref.at[:, to], wgu.at[x, :, :, pl.ds(FE, FE)], wg_s.at[1, d], wg_r.at[1, x], dev)
+        send(up_ref.at[:, to], wgu.at[x, :, :, pl.ds(FE, FE)], wg_s.at[1], wg_r.at[1], dev)
 
     near_x = sorted({1, nx - 1})
     for d in near_x:
@@ -341,7 +338,7 @@
 
     for d in range(1, ny):
         to = (y + d) % ny
-        send(down_ref.at[to], wd.at[y], wd_s.at[d], wd_r.at[y], (z, c, to, x))
+        send(down_ref.at[to], wd.at[y], wd_s.at[0], wd_r.at[0], (z, c, to, x))
 
     local(up_ref.at[:, x], wgu.at[x, :, :, pl.ds(FE, FE)], 3)
     local(down_ref.at[y], wd.at[y], 4)
@@ -359,7 +356,7 @@
         @pl.when((c == i % 2) & (away(i) != 0))
         def _():
             rcopy(
-                dst.at[i], dst.at[i], kv_f.at[part, i, 0], kv_r.at[part, i], (z, 1 - c, y, x)
+                dst.at[i], dst.at[i], kv_f.at[part, i], kv_r.at[part, i], (z, 1 - c, y, x)
             ).start()
 
     def arrive_first(part):
@@ -373,11 +370,11 @@
             @pl.when(hub(i))
             def _():
                 pass_on(part, i)
-                for n, d in ((1, 1), (2, nz - 1)):
+                for d in (1, nz - 1):
                     rcopy(
                         dst.at[i],
                         dst.at[i],
-                        kv_f.at[part, i, n],
+                        kv_f.at[part, i],
                         kv_r.at[part, i],
                         ((z + d) % nz, c, y, x),
                     ).start()
@@ -393,9 +390,7 @@
     arrive_first(0)
     arrive(0)
     arrive_first(1)
-    for d in range(1, grp):
-        g = (j + d) % grp
-        landed(qbuf.at[g], q_r.at[g])
+    landed(qbuf.at[pl.ds(0, grp - 1)], q_r.at[0])
 
     scale_a = HA**-0.5 * LOG2E
     scale_b = HB**-0.5 * LOG2E
@@ -421,7 +416,7 @@
     def hand_over(part, src, dst, d, g):
         @pl.when(d < grp)
         def _():
-            rcopy(src.at[g], dst.at[j], o_s.at[part, g], o_r.at[part, j], member(g)).start()
+            rcopy(src.at[g], dst.at[j], o_s.at[part], o_r.at[part], member(g)).start()
 
         @pl.when(d == grp)
         def _():
@@ -456,14 +451,12 @@
         lsend[g, :, 0:t] = lse_rows[g : g + 1]
     for d in range(1, grp):
         g = (j + d) % grp
-        send(lsend.at[g], lbuf.at[j], o_s.at[2, g], o_r.at[2, j], member(g))
+        send(lsend.at[g], lbuf.at[j], o_s.at[2], o_r.at[2], member(g))
     lbuf[j] = lsend[j]
 
-    for d in range(1, grp):
-        g = (j + d) % grp
-        landed(obl.at[g], o_r.at[0, g])
-        landed(obb.at[g], o_r.at[1, g])
-        landed(lbuf.at[g], o_r.at[2, g])
+    landed(obl.at[pl.ds(0, grp - 1)], o_r.at[0])
+    landed(obb.at[pl.ds(0, grp - 1)], o_r.at[1])
+    landed(lbuf.at[pl.ds(0, grp - 1)], o_r.at[2])
 
     row_g = lax.broadcasted_iota(jnp.int32, (8, t), 0)
     lse_rows = jnp.zeros((8, t), f32)
@@ -498,30 +491,24 @@
     stsend[:, 0:t] = squares[0:2]
     for d in range(1, ntp):
         n = (tp + d) % ntp
-        send(stsend, stbuf.at[tp], st_s.at[d], st_r.at[tp], tp_dev(n))
+        send(stsend, stbuf.at[tp], st_s.at[0], st_r.at[0], tp_dev(n))
     stbuf[tp] = stsend[...]
     for d in range(1, nx):
         to = (x + d) % nx
-        send(msend, mbuf.at[x], m_s.at[d], m_r.at[x], (z, c, y, to))
+        send(msend, mbuf.at[x], m_s.at[0], m_r.at[0], (z, c, y, to))
     mbuf[x] = msend[...]
-    for d in range(1, ntp):
-        n = (tp + d) % ntp
-        landed(stbuf.at[n], st_r.at[n])
+    landed(stbuf.at[pl.ds(0, ntp - 1)], st_r.at[0])
     sums = jnp.sum(stbuf[...], axis=0)[:, 0:t]
     row_t = lax.broadcasted_iota(jnp.int32, (8, t), 0)
     sums = jnp.where(row_t == 0, sums[0:1] * (1.0 / (ntp * HA)), sums[1:2] * (1.0 / (ntp * HB)))
     inverse = lax.rsqrt(sums + epsilon)
     norm_a = dot_exact(inverse, pick_a, first)
     norm_b = dot_exact(inverse, pick_b, first)
-    for d in range(1, nx):
-        n = (x + d) % nx
-        landed(mbuf.at[n], m_r.at[n])
+    landed(mbuf.at[pl.ds(0, nx - 1)], m_r.at[0])
     for copy in locals_:
         copy.wait()
-    for d in range(1, ny):
-        n = (y + d) % ny
-        landed(wo.at[n, :, 1], wo_r.at[0, n])
-        landed(wo.at[n, :, pl.ds(2, 2)], wo_r.at[1, n])
+    landed(wo.at[pl.ds(0, ny - 1), :, 1], wo_r.at[0])
+    landed(wo.at[pl.ds(0, ny - 1), :, pl.ds(2, 2)], wo_r.at[1])
     for n in range(nx):
         gain = mg_ref[pl.ds((y * nx + n) // 2, 1)]
         if n % 2 == 0:
@@ -540,14 +527,14 @@
     for d in range(1, ny):
         to = (y + d) % ny
         psend[d] = project(to).astype(bf16)
-        send(psend.at[d], pbuf.at[y], p_s.at[d], p_r.at[y], (z, c, to, x))
+        send(psend.at[d], pbuf.at[y], p_s.at[0], p_r.at[0], (z, c, to, x))
     for d in range(1, nx):
         if d not in near_x:
             send_up(d)
     total = tok_ref[...].astype(f32) + project(y)
+    landed(pbuf.at[pl.ds(0, ny - 1)], p_r.at[0])
     for d in range(1, ny):
         n = (y + d) % ny
-        landed(pbuf.at[n], p_r.at[n])
         total = total + pbuf[n].astype(f32)
     stream[...] = total
     ones8 = jnp.ones((8, FW), f32)
@@ -555,7 +542,7 @@
     st2send[:, 0:t] = dot_exact(ones8, total * total, last)[0:1]
     for d in range(1, ntp):
         n = (tp + d) % ntp
-        send(st2send, st2buf.at[tp], st2_s.at[d], st2_r.at[tp], tp_dev(n))
+        send(st2send, st2buf.at[tp], st2_s.at[0], st2_r.at[0], tp_dev(n))
     st2buf[tp] = st2send[...]
 
     feats = (total * cg_ref[...]).astype(bf16)
@@ -564,24 +551,21 @@
         outgo[n] = picked[n * cap : (n + 1) * cap]
     near = s // cb
 
-    def dispatch(n):
-        copy = rcopy(outgo.at[n], xbuf.at[y, s], d_s.at[n], d_r.at[s], sp_dev(n))
-        copy.start()
-        return copy
+    def dispatch(n, part):
+        send(outgo.at[n], xbuf.at[y, s], d_s.at[part], d_r.at[near], sp_dev(n))
 
     def dispatch_far(far):
         for i in range(cb):
             for d in sorted({NCH - far, far}, reverse=True):
-                sends.append(dispatch((near + d) % NCH * cb + i))
-
-    for copy in [dispatch(near * cb + (s + d) % cb) for d in range(1, cb)]:
-        copy.wait_send()
+                dispatch((near + d) % NCH * cb + i, 1)
+
+    for d in range(1, cb):
+        dispatch(near * cb + (s + d) % cb, 0)
+    landed(outgo.at[pl.ds(0, cb - 1)], d_s.at[0])
     xbuf[y, s] = outgo[s]
     for far in range(1, NCH // 2):
         dispatch_far(far)
-    for d in range(1, ntp):
-        n = (tp + d) % ntp
-        landed(st2buf.at[n], st2_r.at[n])
+    landed(st2buf.at[pl.ds(0, ntp - 1)], st2_r.at[0])
     squares = jnp.sum(st2buf[...], axis=0)[:, 0:t]
     inverse = lax.rsqrt(squares * (1.0 / (ntp * FW)) + epsilon)
     inverse = jnp.broadcast_to(inverse, (8, t))
@@ -593,7 +577,7 @@
         scsend[n] = factors[:, n * 128 : (n + 1) * 128]
     for d in range(1, nsp):
         n = (s + d) % nsp
-        send(scsend.at[n // per], scbuf.at[s], sc_s.at[d], sc_r.at[s], sp_dev(n))
+        send(scsend.at[n // per], scbuf.at[s], sc_s.at[0], sc_r.at[near], sp_dev(n))
     scbuf[s] = scsend[s // per]
     dispatch_far(NCH // 2)
 
@@ -602,30 +586,20 @@
 
     def stage_a(k):
         ch = chunk(k)
-        for i in range(cb):
-            b = ch * cb + i
-
-            @pl.when(b != s)
-            def _():
-                landed(xbuf.at[y, b], d_r.at[b])
-
+        landed(xbuf.at[y, pl.ds(0, cb - (k == 0))], d_r.at[ch])
         part = xbuf.at[y, pl.ds(ch * cb, cb)]
         for d in range(1, ny):
             to = (y + d) % ny
-            rcopy(part, part, ya_s.at[ch, d], ya_r.at[ch, y], (z, c, to, x)).start()
+            rcopy(part, part, ya_s.at[0], ya_r.at[ch], (z, c, to, x)).start()
 
     def stage_b(k):
         ch = chunk(k)
-        for d in range(1, ny):
-            n = (y + d) % ny
-            landed(xbuf.at[n, pl.ds(ch * cb, cb)], ya_r.at[ch, n])
+        landed(xbuf.at[pl.ds(0, ny - 1), pl.ds(0, cb)], ya_r.at[ch])
 
         @pl.when(k == 0)
         def _():
-            for d in range(1, nx):
-                n = (x + d) % nx
-                landed(wgu.at[n, :, :, pl.ds(0, FE)], wg_r.at[0, n])
-                landed(wgu.at[n, :, :, pl.ds(FE, FE)], wg_r.at[1, n])
+            for n in range(2):
+                landed(wgu.at[pl.ds(0, nx - 1), :, :, pl.ds(n * FE, FE)], wg_r.at[n])
 
         xs = [xbuf[n, pl.ds(ch * cb, cb)].reshape(rows, FW) for n in range(ny)]
 
@@ -639,27 +613,31 @@
             to = (x + d) % nx
             rsend[ch, d] = expand(to).astype(bf16)
             rcopy(
-                rsend.at[ch, d], rbuf.at[ch, x], rx_s.at[ch, d], rx_r.at[ch, x], (z, c, y, to)
+                rsend.at[ch, d], rbuf.at[ch, x], rx_s.at[0], rx_r.at[ch], (z, c, y, to)
             ).start()
         gown[ch] = expand(x)
 
     def stage_c(k):
         ch = chunk(k)
         both = gown[ch]
+        landed(rbuf.at[ch, pl.ds(0, nx - 1)], rx_r.at[ch])
         for d in range(1, nx):
             n = (x + d) % nx
-            landed(rbuf.at[ch, n], rx_r.at[ch, n])
             both = both + rbuf[ch, n].astype(f32)
         row = lax.broadcasted_iota(jnp.int32, (cap, 128), 0)
         spot = row + s % per * wide == lax.broadcasted_iota(jnp.int32, (cap, 128), 1)
         factor = []
+
+        @pl.when(k == 0)
+        def _():
+            landed(scbuf.at[pl.ds(0, cb - 1)], sc_r.at[ch])
+
+        @pl.when(k > 0)
+        def _():
+            landed(scbuf.at[pl.ds(0, cb)], sc_r.at[ch])
+
         for i in range(cb):
             b = ch * cb + i
-
-            @pl.when(b != s)
-            def _():
-                landed(scbuf.at[b], sc_r.at[b])
-
             value = jnp.where(spot, scbuf[b], 0.0)
             factor.append(jnp.sum(value, axis=1, keepdims=True))
         both = both * jnp.concatenate(factor, axis=0)
@@ -669,36 +647,32 @@
         for d in range(1, nx):
             to = (x + d) % nx
             rcopy(
-                hbuf.at[ch, x], hbuf.at[ch, x], hx_s.at[ch, d], hx_r.at[ch, x], (z, c, y, to)
+                hbuf.at[ch, x], hbuf.at[ch, x], hx_s.at[0], hx_r.at[ch], (z, c, y, to)
             ).start()
 
     def stage_d(k):
         ch = chunk(k)
-        for d in range(1, nx):
-            n = (x + d) % nx
-            landed(hbuf.at[ch, n], hx_r.at[ch, n])
+        landed(hbuf.at[ch, pl.ds(0, nx - 1)], hx_r.at[ch])
 
         @pl.when(k == 0)
         def _():
-            for d in range(1, ny):
-                n = (y + d) % ny
-                landed(wd.at[n], wd_r.at[n])
+            landed(wd.at[pl.ds(0, ny - 1)], wd_r.at[0])
 
         wide = jnp.concatenate([hbuf[ch, n] for n in range(nx)], axis=1)
         for d in range(1, ny):
             to = (y + d) % ny
             dsend[ch, d] = dot_n(wide, wd[to]).astype(bf16)
             rcopy(
-                dsend.at[ch, d], dbuf.at[ch, y], ry_s.at[ch, d], ry_r.at[ch, y], (z, c, to, x)
+                dsend.at[ch, d], dbuf.at[ch, y], ry_s.at[0], ry_r.at[ch], (z, c, to, x)
             ).start()
         down_own[ch] = dot_n(wide, wd[y])
 
     def stage_e(k):
         ch = chunk(k)
         acc = down_own[ch]
+        landed(dbuf.at[ch, pl.ds(0, ny - 1)], ry_r.at[ch])
         for d in range(1, ny):
             n = (y + d) % ny
-            landed(dbuf.at[ch, n], ry_r.at[ch, n])
             acc = acc + dbuf[ch, n].astype(f32)
         eout[pl.ds(ch * cb, cb)] = acc.astype(bf16).reshape(cb, cap, FW)
         for i in range(cb):
@@ -706,7 +680,7 @@
 
             @pl.when(b != s)
             def _():
-                rcopy(eout.at[b], ret.at[s], b_s.at[b], b_r.at[s], sp_dev(b)).start()
+                rcopy(eout.at[b], ret.at[s], b_s.at[0], b_r.at[0], sp_dev(b)).start()
 
             @pl.when(b == s)
             def _():
@@ -715,35 +689,26 @@
 
     stages = (stage_a, stage_b, stage_c, stage_d, stage_e)
 
-    ahead = ((1, 1), (1, 2)) if NCH == 4 else ()
-    behind = ((0, 0), (2, 3)) if NCH == 4 else tuple((k, k) for k in range(NCH))
+    behind = ((0, 0), (1, 1), (1, 2), (2, 3)) if NCH == 4 else tuple((k, k) for k in range(NCH))
 
     def step(i, carry):
-        for at, k in ahead:
+        for lag in (4, 3, 2, 1):
+
+            @pl.when((i >= lag) & (i < NCH + lag))
+            def _():
+                stages[lag](i - lag)
+
+        for at, k in behind:
 
             @pl.when(i == at)
             def _():
                 stage_a(k)
 
-        for lag in (4, 3, 2, 1):
-
-            @pl.when((i >= lag) & (i < NCH + lag))
-            def _():
-                stages[lag](i - lag)
-
-        for at, k in behind:
-
-            @pl.when(i == at)
-            def _():
-                stage_a(k)
-
         return carry
 
     lax.fori_loop(0, NCH + len(stages) - 1, step, 0)
 
-    for d in range(1, nsp):
-        n = (s + d) % nsp
-        landed(ret.at[n], b_r.at[n])
+    landed(ret.at[pl.ds(0, nsp - 1)], b_r.at[0])
     back = ret[...].reshape(nsp * cap, FW)
     gap = rl_ref[0:1] - rl_ref[1:2]
     w0 = gw_ref[...] / (1.0 + jnp.exp(-gap))
@@ -754,42 +719,43 @@
     routed = w0 * flipped(sel0[...], back) + w1 * flipped(sel1[...], back)
     o_ref[...] = (stream[...] + routed).astype(bf16)
 
-    for copy in sends:
-        copy.wait_send()
 
     for part, (src, dst) in enumerate(kv_pairs):
 
         @pl.when(source)
         def _():
-            for n in (*range(len(hubs)), nz - 1):
-                landed(src, kv_s.at[part, n])
+            landed(dst.at[pl.ds(0, len(hubs) + 1)], kv_s.at[part])
 
         for i in range(nb):
-            relay = (c == i % 2) & (z != (i * grp + j) // 2)
-
-            @pl.when(relay)
-            def _():
-                landed(dst.at[i], kv_f.at[part, i, 0])
 
             @pl.when(hub(i))
             def _():
-                for n in (1, 2):
-                    landed(dst.at[i], kv_f.at[part, i, n])
-
-    for d in range(1, grp):
-        g = (j + d) % grp
-        landed(osl.at[g], o_s.at[0, g])
-        landed(osb.at[g], o_s.at[1, g])
-    for ch in range(NCH):
-        for d in range(1, ny):
-            landed(xbuf.at[y, pl.ds(ch * cb, cb)], ya_s.at[ch, d])
-            landed(dsend.at[ch, d], ry_s.at[ch, d])
-        for d in range(1, nx):
-            landed(rsend.at[ch, d], rx_s.at[ch, d])
-            landed(hbuf.at[ch, x], hx_s.at[ch, d])
-    for d in range(1, nsp):
-        b = (s + d) % nsp
-        landed(eout.at[b], b_s.at[b])
+                landed(dst.at[pl.ds(0, min(3, nb))], kv_f.at[part, i])
+
+            @pl.when((c == i % 2) & (away(i) != 0) & jnp.logical_not(hub(i)))
+            def _():
+                landed(dst.at[i], kv_f.at[part, i])
+
+    landed(qbuf.at[pl.ds(0, grp - 1)], q_s.at[0])
+    for n in range(2):
+        landed(((obl, obb)[n]).at[pl.ds(0, grp - 1)], o_s.at[n])
+    landed(lbuf.at[pl.ds(0, grp - 1)], o_s.at[2])
+    landed(wo.at[pl.ds(0, ny - 1), :, 1], wo_s.at[0])
+    landed(wo.at[pl.ds(0, ny - 1), :, pl.ds(2, 2)], wo_s.at[1])
+    for n in range(2):
+        landed(wgu.at[pl.ds(0, nx - 1), :, :, pl.ds(n * FE, FE)], wg_s.at[n])
+    landed(wd.at[pl.ds(0, ny - 1)], wd_s.at[0])
+    landed(mbuf.at[pl.ds(0, nx - 1)], m_s.at[0])
+    landed(stbuf.at[pl.ds(0, ntp - 1)], st_s.at[0])
+    landed(pbuf.at[pl.ds(0, ny - 1)], p_s.at[0])
+    landed(st2buf.at[pl.ds(0, ntp - 1)], st2_s.at[0])
+    landed(outgo.at[pl.ds(0, nsp - cb)], d_s.at[1])
+    landed(scbuf.at[pl.ds(0, nsp - 1)], sc_s.at[0])
+    landed(xbuf.at[pl.ds(0, ny - 1)], ya_s.at[0])
+    landed(rbuf.at[:, pl.ds(0, nx - 1)], rx_s.at[0])
+    landed(hbuf.at[:, pl.ds(0, nx - 1)], hx_s.at[0])
+    landed(dbuf.at[:, pl.ds(0, ny - 1)], ry_s.at[0])
+    landed(ret.at[pl.ds(0, nsp - 1)], b_s.at[0])
 
 
 def on_device(
@@ -872,42 +838,42 @@
             pltpu.VMEM((NCH, rows, FW), f32),
             pltpu.VMEM((nsp, cap, FW), bf16),
             pltpu.VMEM((nsp, cap, FW), bf16),
-            dma((grp,)),
-            dma((grp,)),
-            dma((2, nz)),
+            dma((1,)),
+            dma((1,)),
+            dma((2,)),
             dma((2, nb)),
-            dma((2, nb, 3)),
-            dma((3, grp)),
-            dma((3, grp)),
-            dma((2, ny)),
-            dma((2, ny)),
-            dma((2, nx)),
-            dma((2, nx)),
-            dma((ny,)),
-            dma((ny,)),
+            dma((2, nb)),
+            dma((3,)),
+            dma((3,)),
+            dma((2,)),
+            dma((2,)),
+            dma((2,)),
+            dma((2,)),
+            dma((1,)),
+            dma((1,)),
             dma((5,)),
-            dma((nx,)),
-            dma((nx,)),
-            dma((ntp,)),
-            dma((ntp,)),
-            dma((ny,)),
-            dma((ny,)),
-            dma((ntp,)),
-            dma((ntp,)),
-            dma((nsp,)),
-            dma((nsp,)),
-            dma((nsp,)),
-            dma((nsp,)),
-            dma((NCH, ny)),
-            dma((NCH, ny)),
-            dma((NCH, nx)),
-            dma((NCH, nx)),
-            dma((NCH, nx)),
-            dma((NCH, nx)),
-            dma((NCH, ny)),
-            dma((NCH, ny)),
-            dma((nsp,)),
-            dma((nsp,)),
+            dma((1,)),
+            dma((1,)),
+            dma((1,)),
+            dma((1,)),
+            dma((1,)),
+            dma((1,)),
+            dma((1,)),
+            dma((1,)),
+            dma((2,)),
+            dma((NCH,)),
+            dma((1,)),
+            dma((NCH,)),
+            dma((1,)),
+            dma((NCH,)),
+            dma((1,)),
+            dma((NCH,)),
+            dma((1,)),
+            dma((NCH,)),
+            dma((1,)),
+            dma((NCH,)),
+            dma((1,)),
+            dma((1,)),
         ],
         compiler_params=pltpu.CompilerParams(
             collective_id=0, has_side_effects=True, vmem_limit_bytes=60 * 1024 * 1024

time: 146 us -> 139 us (0.952)
  Pallas kernels: 144 us -> 138 us
    pallas_call x1, Pallas kernels: 144 us -> 138 us  [on_device(): pl.pallas_call(functools.partial(layer_kernel, (nz, ny, nx, t, cap)), out...]
where the time goes in v4:
time: 139 us
  Pallas kernels  138 us (99%)
  local copies, waits for them, and re-layouts  1.54 us (1%)
    pallas_call x1, Pallas kernels, on_device(): pl.pallas_call(functools.partial(layer_kernel, (nz, ny, nx, t, cap)), out...  138 us

profile of v4, /device:TPU:1, one launch (start us, length us, event | category | flops | bytes accessed | tf_op | source)
XLA Modules:
  0.0 139.2 jit_solution(12819757596150290867)
XLA Ops:
  0.0 137.7 %shard_map.172 = bf16[192,256]{1,0:T(8,128)(2,1)} custom-call(bf16[64,192]{1,0:T(8,128)(2,1)} %bitcast.28, bf16[2,64,192]{2,1,0:T(8,128)(2,1)} %bitcast.25, bf16[2,64,192]{2,1,0:T(8,128)(2,1)} %bitcast.26, f32[2,64]{1,0:T(2,128)} %lg_ref.1, bf16[192,128]{1,0:T(8,128)(2,1)} %bitcast.27, bf16[384,128]{1,0:T(8,128)(2,1)} %bitcast.23, ...), custom_call_target="tpu_custom_call" | custom-call | tf_op jit(solution)/shard_map/pallas_call | solution.py:795
  137.7 1.5 %copy.20 = bf16[192,256]{1,0:T(8,128)(2,1)} copy(bf16[192,256]{1,0:T(8,128)(2,1)} %shard_map.172) | data formatting | bytes 196608

commit v5 on v4

--- a/solution.py
+++ b/solution.py
@@ -17,7 +17,7 @@
 NY, NX = 4, 4
 NCH = 4
 HUBS = (8, 5, 11, 2, 14)
-UNROLL = 2
+UNROLL = 4
 HA, HB = 64, 128
 FW = 256
 FE = 128
@@ -62,6 +62,7 @@
 
 def layer_kernel(
     dims,
+    loads,
     lq_ref,
     lk_ref,
     lv_ref,
@@ -192,6 +193,9 @@
     for d in range(1, ntp):
         pl.semaphore_signal(barrier, inc=1, device_id=tp_dev((tp + d) % ntp), device_id_type=MESH)
 
+    for copy in loads:
+        copy.wait()
+
     def turned(raw, swapped, gain, size):
         quarter = size // 4
         lane = lax.broadcasted_iota(jnp.int32, (t, 128), 1)
@@ -388,8 +392,8 @@
                 pass_on(part, i)
 
     arrive_first(0)
+    arrive_first(1)
     arrive(0)
-    arrive_first(1)
     landed(qbuf.at[pl.ds(0, grp - 1)], q_r.at[0])
 
     scale_a = HA**-0.5 * LOG2E
@@ -717,7 +721,7 @@
     w0, w1 = dot_exact(both, pick_a, first), dot_exact(both, pick_b, first)
     w0, w1 = jnp.concatenate([w0, w0], axis=1), jnp.concatenate([w1, w1], axis=1)
     routed = w0 * flipped(sel0[...], back) + w1 * flipped(sel1[...], back)
-    o_ref[...] = (stream[...] + routed).astype(bf16)
+    o_ref[...] = stream[...] + routed
 
 
     for part, (src, dst) in enumerate(kv_pairs):
@@ -756,6 +760,20 @@
     landed(hbuf.at[:, pl.ds(0, nx - 1)], hx_s.at[0])
     landed(dbuf.at[:, pl.ds(0, ny - 1)], ry_s.at[0])
     landed(ret.at[pl.ds(0, nsp - 1)], b_s.at[0])
+
+
+SMALL = (*range(9), *range(14, 19))
+
+
+def entry(dims, *refs):
+    inputs, rest = list(refs[:19]), refs[19 : -len(SMALL) - 1]
+    loads = []
+    for n, (i, held) in enumerate(zip(SMALL, refs[-len(SMALL) - 1 : -1])):
+        copy = pltpu.make_async_copy(inputs[i], held, refs[-1].at[n])
+        copy.start()
+        loads.append(copy)
+        inputs[i] = held
+    layer_kernel(dims, loads, *inputs, *rest)
 
 
 def on_device(
@@ -792,10 +810,31 @@
     vm = pl.BlockSpec(memory_space=pltpu.VMEM)
     hbm = pl.BlockSpec(memory_space=pl.ANY)
     dma = pltpu.SemaphoreType.DMA
+    inputs = (
+        lean_query.transpose(1, 2, 0)[0],
+        lean_key.transpose(1, 2, 0),
+        lean_value.transpose(1, 2, 0),
+        lean_gains,
+        broad_query[:, 0],
+        broad_key.reshape(KV * t, HB),
+        broad_value.reshape(KV * t, HB),
+        broad_gains,
+        tokens,
+        output_weight.reshape(3 * ntp, 64, FW),
+        output_weight.reshape(3 * ntp // 2, 2, 64, FW),
+        gate_weight.reshape(ny, nx, FW, FE),
+        up_weight.reshape(ny, nx, FW, FE),
+        down_weight.reshape(ny, nx * FE, FW),
+        mixer_gain.reshape(-1, 128),
+        channel_gain.reshape(1, FW),
+        route_experts.T,
+        route_logits.T,
+        group_weight.reshape(1, t),
+    )
     return pl.pallas_call(
-        functools.partial(layer_kernel, (nz, ny, nx, t, cap)),
-        out_shape=jax.ShapeDtypeStruct((t, FW), bf16),
-        in_specs=[vm] * 9 + [hbm] * 5 + [vm] * 5,
+        functools.partial(entry, (nz, ny, nx, t, cap)),
+        out_shape=jax.ShapeDtypeStruct((t, FW), f32),
+        in_specs=[hbm] * 19,
         out_specs=vm,
         scratch_shapes=[
             pltpu.VMEM((t, 256), bf16),
@@ -874,31 +913,13 @@
             dma((NCH,)),
             dma((1,)),
             dma((1,)),
+            *(pltpu.VMEM(inputs[i].shape, inputs[i].dtype) for i in SMALL),
+            dma((len(SMALL),)),
         ],
         compiler_params=pltpu.CompilerParams(
             collective_id=0, has_side_effects=True, vmem_limit_bytes=60 * 1024 * 1024
         ),
-    )(
-        lean_query.transpose(1, 2, 0)[0],
-        lean_key.transpose(1, 2, 0),
-        lean_value.transpose(1, 2, 0),
-        lean_gains,
-        broad_query[:, 0],
-        broad_key.reshape(KV * t, HB),
-        broad_value.reshape(KV * t, HB),
-        broad_gains,
-        tokens,
-        output_weight.reshape(3 * ntp, 64, FW),
-        output_weight.reshape(3 * ntp // 2, 2, 64, FW),
-        gate_weight.reshape(ny, nx, FW, FE),
-        up_weight.reshape(ny, nx, FW, FE),
-        down_weight.reshape(ny, nx * FE, FW),
-        mixer_gain.reshape(-1, 128),
-        channel_gain.reshape(1, FW),
-        route_experts.T,
-        route_logits.T,
-        group_weight.reshape(1, t),
-    )
+    )(*inputs).astype(bf16)
 
 
 def solution(mesh):

time: 139 us -> 138 us (level)
  Pallas kernels: 138 us -> 136 us
  other arithmetic: 0 us -> 1.58 us
  local copies, waits for them, and re-layouts: 1.54 us -> 0 us
    pallas_call x1, Pallas kernels: 138 us -> 136 us  [on_device(): pl.pallas_call(functools.partial(entry, (nz, ny, nx, t, cap)), out_shape=...]
    convert_element_type x0 -> x1, other arithmetic: none -> 1.58 us  [on_device(): return pl.pallas_call(functools.partial(entry, (nz, ny, nx, t, cap)), out...]
    unnamed x1 -> x0, local copies, waits for them, and re-layouts: 1.54 us -> none
where the time goes in v5:
time: 138 us; the launch traced here: 137 us
  Pallas kernels  136 us (99%)
  other arithmetic  1.58 us (1%)
    pallas_call x1, Pallas kernels, on_device(): pl.pallas_call(functools.partial(entry, (nz, ny, nx, t, cap)), out_shape=...  136 us

profile of v5, /device:TPU:1, one launch (start us, length us, event | category | flops | bytes accessed | tf_op | source)
XLA Modules:
  0.0 137.3 jit_solution(7280547172927186640)
XLA Ops:
  0.0 135.7 %shard_map.172 = f32[192,256]{1,0:T(8,128)} custom-call(bf16[64,192]{1,0:T(8,128)(2,1)} %bitcast.28, bf16[2,64,192]{2,1,0:T(8,128)(2,1)} %bitcast.25, bf16[2,64,192]{2,1,0:T(8,128)(2,1)} %bitcast.26, f32[2,64]{1,0:T(2,128)} %refs_3_.1, bf16[192,128]{1,0:T(8,128)(2,1)} %bitcast.27, bf16[384,128]{1,0:T(8,128)(2,1)} %bitcast.23, bf16[384,128]{1,0:T(8,128)(2,1)} %bitcast.24, ...), custom_call_target="tpu_custom_call" | custom-call | tf_op jit(solution)/shard_map/pallas_call | solution.py:834
  135.7 1.6 %convert_element_type.3 = bf16[192,256]{1,0:T(8,128)(2,1)} convert(f32[192,256]{1,0:T(8,128)} %shard_map.172) | non-fusion elementwise | flops 49152 | bytes 294912 | tf_op jit(solution)/shard_map/convert_element_type | solution.py:922
